TPU v7x, 256 devices: a 4x2x16 block of a 4x16x16 slice. The times are simulated.
256 devices in a mesh: grp: 2 (over y), sp: 16 (over z), tp: 4 (over x), dp: 2 (over core).
Axes of the slice: x: 4, y: 2, z: 16, core: 2. Of those that a mesh axis runs over, the one named last changes fastest.
The devices are a block of a 4x16x16 slice.
Arguments:
- latent: bfloat16 [4, 6144, 2048], P(('grp', 'dp'), ('sp', 'tp')), parts along dimension 0, may hold values from -6 to 6
- cond: bfloat16 [4, 2048], P(('grp', 'dp')), parts along dimension 0, may hold values from -6 to 6
- context: bfloat16 [4, 256, 2048], P(('grp', 'dp'), 'sp'), parts along dimension 0, may hold values from -6 to 6
- cond_ctx: bfloat16 [2048], replicated, may hold values from -8 to 8
- w_shift: bfloat16 [2048, 2048], P('sp', 'tp'), may hold values from -0.125 to 0.125
- w_scale: bfloat16 [2048, 2048], P('sp', 'tp'), may hold values from -0.125 to 0.125
- w_gate: bfloat16 [2048, 2048], P('sp', 'tp'), may hold values from -0.125 to 0.125
- norm_gain: float32 [2048], replicated, may hold values from 0.1 to 1.9
- w_query: bfloat16 [2048, 1024], P(None, 'tp'), may hold values from -0.125 to 0.125
- w_key: bfloat16 [2048, 512], P(None, 'tp'), may hold values from -0.125 to 0.125
- w_value: bfloat16 [2048, 512], P(None, 'tp'), may hold values from -0.125 to 0.125
- query_gain: float32 [128], replicated, may hold values from 0.6 to 16
- key_gain: float32 [128], replicated, may hold values from 0.6 to 16
- ctx_lift: float32 [8], P('tp'), may hold values from -2 to 0.5
- out_gain: float32 [1024], replicated, may hold values from 0.1 to 1.9
- w_out: bfloat16 [1024, 2048], replicated, may hold values from -0.1875 to 0.1875
Outputs:
- result: bfloat16 [4, 6144, 2048], P(('grp', 'dp'), ('sp', 'tp')), parts along dimension 0
There are 2 independent parts, one for each index of `grp`. A program takes and returns all parts, laid end to end along the dimension named above; an argument that names none is the same for every part. Nothing has to cross between parts.
All inputs are finite; a program needn't handle non-finite values.
Results may differ from a plain program's by a relative error of at most 0.023.
The roundings to bfloat16 on the way count: a program that leaves them out, or rounds other values in their place, can miss the bound.
Values may be sent and summed in bfloat16 or wider, within the bound.
A program may use at most 64 MiB of HBM per device.

v0:
```python
import math

import jax
import jax.numpy as jnp
from jax import lax
from jax.sharding import PartitionSpec as P

HEADS = 8
KV_HEADS = 4
HEAD_DIM = 128
GRID_WIDTH = 64


EPSILON = 1e-06


def copy_for_each(x, axis):
    count = lax.axis_size(axis)
    return lax.all_to_all(jnp.broadcast_to(x[None], (count, *x.shape)), axis, 0, 0, tiled=True)


def over_copies(x, axis):
    return copy_for_each(x, axis).sum(axis=0)


def laid_out(tiles, dim):
    tiles = jnp.moveaxis(tiles, 0, dim)
    dims = tiles.shape
    return tiles.reshape(*dims[:dim], dims[dim] * dims[dim + 1], *dims[dim + 2 :])


def collect(x, axis, dim):
    return laid_out(copy_for_each(x, axis), dim)


def side_by_side(arrays, axis, dim, along):
    ends, at = ([], 0)
    for a in arrays[:-1]:
        at += a.shape[along]
        ends.append(at)
    both = jnp.concatenate(arrays, axis=along)
    return tuple(jnp.split(lax.all_gather(both, axis, axis=dim, tiled=True), ends, axis=along))


def rotate(vectors, positions):
    freqs = vectors.shape[-1] // 4
    grid_rows = (positions // GRID_WIDTH).astype(jnp.float32)
    grid_cols = (positions % GRID_WIDTH).astype(jnp.float32)
    inverse = 10000.0 ** (-jnp.arange(freqs, dtype=jnp.float32) / freqs)
    angles = jnp.stack([grid_rows[:, None] * inverse, grid_cols[:, None] * inverse], axis=1)
    cosine = jnp.cos(angles)[:, None]
    sine = jnp.sin(angles)[:, None]
    split = vectors.reshape(vectors.shape[:-1] + (2, 2, freqs))
    first = split[..., 0, :]
    second = split[..., 1, :]
    return jnp.stack(
        [first * cosine - second * sine, second * cosine + first * sine], axis=-2
    ).reshape(vectors.shape)


def head_norm(vectors, gain_vector):
    floats = vectors.astype(jnp.float32)
    return floats * lax.rsqrt(jnp.mean(floats * floats, -1, keepdims=True) + EPSILON) * gain_vector


def modulated_norm(row_data, gain_vector, shift_row, scale_row):
    floats = row_data.astype(jnp.float32)
    normal = floats * lax.rsqrt(jnp.mean(floats * floats, -1, keepdims=True) + EPSILON)
    return (normal * gain_vector * (1.0 + scale_row) + shift_row).astype(jnp.bfloat16)


def on_device(
    latent,
    cond,
    context,
    cond_ctx,
    w_shift,
    w_scale,
    w_gate,
    norm_gain,
    w_query,
    w_key,
    w_value,
    query_gain,
    key_gain,
    ctx_lift,
    out_gain,
    w_out,
):
    sp_index = lax.axis_index("sp")
    in_rows = w_shift.shape[0]
    sources = jnp.concatenate([cond, cond_ctx[None]], 0)
    own_inputs = lax.dynamic_slice_in_dim(sources, sp_index * in_rows, in_rows, 1)
    activated = jax.nn.silu(own_inputs.astype(jnp.float32)).astype(jnp.bfloat16)
    partial_mod = jnp.stack(
        [
            jnp.dot(activated, matrix, preferred_element_type=jnp.float32)
            for matrix in (w_shift, w_scale, w_gate)
        ]
    )
    summed_mod = over_copies(partial_mod, "sp")
    modulation = collect(summed_mod, "tp", 2)
    shift_rows = modulation[0]
    scale_rows = modulation[1]
    gate_rows = modulation[2]
    normed = modulated_norm(latent, norm_gain, shift_rows[0], scale_rows[0])
    query_cols = w_query.shape[1]
    key_cols = w_key.shape[1]
    joined_weights = jnp.concatenate([w_query, w_key, w_value], 1)
    projected = jnp.einsum(
        "bsd,de->bse", collect(normed, "tp", 1), joined_weights, preferred_element_type=jnp.float32
    ).astype(jnp.bfloat16)
    seq_rows = projected.shape[1]
    kv_local = key_cols // HEAD_DIM
    group = HEADS // KV_HEADS
    positions = sp_index * seq_rows + jnp.arange(seq_rows, dtype=jnp.int32)
    query_rows = rotate(
        head_norm(
            projected[..., :query_cols].reshape(1, seq_rows, kv_local * group, HEAD_DIM), query_gain
        ),
        positions,
    )
    query_rows = query_rows.astype(jnp.bfloat16).reshape(1, seq_rows, kv_local, group, HEAD_DIM)
    key_rows = rotate(
        head_norm(
            projected[..., query_cols : query_cols + key_cols].reshape(
                1, seq_rows, kv_local, HEAD_DIM
            ),
            key_gain,
        ),
        positions,
    )
    key_rows = key_rows.astype(jnp.bfloat16).reshape(1, seq_rows, key_cols)
    value_rows = projected[..., query_cols + key_cols :]
    ctx_local = context.shape[1]
    lift_table = (ctx_lift + math.log(seq_rows / ctx_local)).reshape(kv_local, group)
    factor = HEAD_DIM ** (-0.5)
    initial = (
        jnp.full((1, kv_local, group, seq_rows), -jnp.inf, jnp.float32),
        jnp.zeros((1, kv_local, group, seq_rows), jnp.float32),
        jnp.zeros((1, kv_local, group, seq_rows, HEAD_DIM), jnp.float32),
    )
    ctx_in_shard = 0
    ctx_normed = modulated_norm(context, norm_gain, shift_rows[1], scale_rows[1])
    ctx_count = context.shape[1]
    ctx_key_rows = jnp.einsum(
        "bsd,de->bse", ctx_normed, w_key, preferred_element_type=jnp.float32
    ).astype(jnp.bfloat16)
    ctx_key_rows = (
        head_norm(ctx_key_rows.reshape(1, ctx_count, kv_local, HEAD_DIM), key_gain)
        .astype(jnp.bfloat16)
        .reshape(1, ctx_count, key_cols)
    )
    ctx_value_rows = jnp.einsum(
        "bsd,de->bse", ctx_normed, w_value, preferred_element_type=jnp.float32
    ).astype(jnp.bfloat16)
    send_keys = jnp.concatenate([ctx_key_rows, key_rows], 1)
    send_values = jnp.concatenate([ctx_value_rows, value_rows], 1)
    shard_length = seq_rows + ctx_local
    ctx_in_shard = ctx_local
    pieces = side_by_side((send_keys, send_values), "sp", 1, 0)
    count = pieces[0].shape[1]
    places = jnp.arange(count, dtype=jnp.int32) % shard_length
    ctx_flags = (places < ctx_in_shard).astype(jnp.float32)
    carried = initial
    key_block = pieces[0]
    value_block = pieces[1]
    count = key_block.shape[1]
    span = max(seq_rows, 512)
    for begin in range(0, count, span):
        finish = min(begin + span, count)
        absorb_key_block = key_block[:, begin:finish]
        absorb_value_block = value_block[:, begin:finish]
        absorb_ctx_flags = ctx_flags[begin:finish]
        running_max, running_sum, weighted = carried
        absorb_count = absorb_key_block.shape[1]
        key_heads = absorb_key_block.reshape(1, absorb_count, kv_local, HEAD_DIM)
        value_heads = absorb_value_block.reshape(1, absorb_count, kv_local, HEAD_DIM)
        scores = (
            jnp.einsum(
                "bqkgd,bnkd->bkgqn", query_rows, key_heads, preferred_element_type=jnp.float32
            )
            * factor
        )
        scores = (
            scores
            + absorb_ctx_flags[None, None, None, None, :] * lift_table[None, :, :, None, None]
        )
        new_max = jnp.maximum(running_max, jnp.max(scores, -1))
        keep_factor = jnp.exp(running_max - new_max)
        exp_scores = jnp.exp(scores - new_max[..., None])
        running_sum = running_sum * keep_factor + jnp.sum(exp_scores, -1)
        weighted = weighted * keep_factor[..., None] + jnp.einsum(
            "bkgqn,bnkd->bkgqd",
            exp_scores.astype(jnp.bfloat16),
            value_heads,
            preferred_element_type=jnp.float32,
        )
        carried = (new_max, running_sum, weighted)
    final_max, final_sum, final_weighted = carried
    attended = final_weighted / final_sum[..., None]
    attended = (
        jnp.transpose(attended, (0, 3, 1, 2, 4))
        .reshape(1, seq_rows, query_cols)
        .astype(jnp.bfloat16)
    )
    token_rows = lax.all_to_all(attended, "tp", split_axis=1, concat_axis=2, tiled=True)
    att_normed = head_norm(token_rows, out_gain).astype(jnp.bfloat16)
    mixture = jnp.einsum("bsd,de->bse", att_normed, w_out, preferred_element_type=jnp.float32)
    return (latent.astype(jnp.float32) + gate_rows[0] * mixture).astype(jnp.bfloat16)


def solution(mesh):
    in_specs = (
        P(("grp", "dp"), ("sp", "tp"), None),
        P(("grp", "dp"), None),
        P(("grp", "dp"), "sp", None),
        P(),
        P("sp", "tp"),
        P("sp", "tp"),
        P("sp", "tp"),
        P(),
        P(None, "tp"),
        P(None, "tp"),
        P(None, "tp"),
        P(),
        P(),
        P("tp"),
        P(),
        P(),
    )
    out_specs = P(("grp", "dp"), ("sp", "tp"), None)
    return jax.shard_map(
        on_device, mesh=mesh, in_specs=in_specs, out_specs=out_specs, check_vma=False
    )
```

profile of v0, /device:TPU:40, one launch (start us, length us, event | category | flops | bytes accessed | tf_op | source)
XLA Modules:
  0.0 198.7 jit_solution(14847287500147752074)
XLA Ops:
  6.6 0.8 broadcast_in_dim.14
  7.5 0.8 convolution_bitcast_fusion
  8.3 1.1 convolution_bitcast_fusion.1
  9.4 1.1 convolution_bitcast_fusion.2
  10.6 0.7 broadcast_in_dim.15
  11.3 24.0 %all-to-all-start = ((f32[16,3,2,512]{3,2,1,0:T(2,128)}), f32[16,3,2,512]{3,2,1,0:T(2,128)S(1)}, u32[]{:S(2)}, u32[]{:S(2)}) async-start(f32[16,3,2,512]{3,2,1,0:T(2,128)} %broadcast_in_dim.15), calls=%async_computation | async-start | bytes 393216 | tf_op jit(solution)/shard_map/all_to_all | solution.py:19
  35.3 1.0 fusion.106
  36.3 1.2 fusion.57
  37.4 14.0 %all-to-all-done = f32[16,3,2,512]{3,2,1,0:T(2,128)S(1)} async-done(((f32[16,3,2,512]{3,2,1,0:T(2,128)}), f32[16,3,2,512]{3,2,1,0:T(2,128)S(1)}, u32[]{:S(2)}, u32[]{:S(2)}) %all-to-all-start) | async-done | bytes 196640 | tf_op jit(solution)/shard_map/all_to_all | solution.py:19
  51.5 0.6 broadcast_in_dim.16
  52.2 4.6 %all-to-all-start.1 = ((f32[4,3,2,512]{3,2,1,0:T(2,128)}), f32[4,3,2,512]{3,2,1,0:T(2,128)S(1)}, u32[]{:S(2)}, u32[]{:S(2)}) async-start(f32[4,3,2,512]{3,2,1,0:T(2,128)} %broadcast_in_dim.16), calls=%async_computation.1 | async-start | bytes 98304 | tf_op jit(solution)/shard_map/all_to_all | solution.py:19
  56.8 5.5 %all-to-all-done.1 = f32[4,3,2,512]{3,2,1,0:T(2,128)S(1)} async-done(((f32[4,3,2,512]{3,2,1,0:T(2,128)}), f32[4,3,2,512]{3,2,1,0:T(2,128)S(1)}, u32[]{:S(2)}, u32[]{:S(2)}) %all-to-all-start.1) | async-done | bytes 49184 | tf_op jit(solution)/shard_map/all_to_all | solution.py:19
  62.6 1.3 broadcast_in_dim.19
  63.9 3.8 %all-to-all-start.2 = ((bf16[4,1,96,2048]{3,2,1,0:T(8,128)(2,1)}), bf16[4,1,96,2048]{3,2,1,0:T(8,128)(2,1)S(1)}, u32[]{:S(2)}, u32[]{:S(2)}) async-start(bf16[4,1,96,2048]{3,2,1,0:T(8,128)(2,1)} %broadcast_in_dim.19), calls=%async_computation.2 | async-start | bytes 3145728 | tf_op jit(solution)/shard_map/all_to_all | solution.py:19
  67.8 0.7 mul.954
  68.5 0.7 fusion.122
  69.9 13.2 %all-to-all-done.2 = bf16[4,1,96,2048]{3,2,1,0:T(8,128)(2,1)S(1)} async-done(((bf16[4,1,96,2048]{3,2,1,0:T(8,128)(2,1)}), bf16[4,1,96,2048]{3,2,1,0:T(8,128)(2,1)S(1)}, u32[]{:S(2)}, u32[]{:S(2)}) %all-to-all-start.2) | async-done | bytes 1572896 | tf_op jit(solution)/shard_map/all_to_all | solution.py:19
  83.1 2.2 %fusion.38 = bf16[1,384,512]{2,1,0:T(8,128)(2,1)S(1)} fusion(bf16[384,2048]{1,0:T(8,128)(2,1)S(1)} %bitcast.325, bf16[2048,128]{1,0:T(8,128)(2,1)S(1)} %copy-done.5, bf16[2048,128]{1,0:T(8,128)(2,1)S(1)} %copy-done.4, bf16[2048,256]{1,0:T(8,128)(2,1)} %param.24), kind=kOutput, calls=%fused_computation.63 | convolution fusion | flops 811794432 | bytes 4063232 | tf_op jit(solution)/shard_map/bsd,de->bse/dot_general | solution.py:110
  85.7 0.8 multiply_multiply_fusion.1
  86.4 1.2 subtract_convert_fusion.1
  87.8 0.7 maximum_maximum_fusion
  89.7 0.5 reduce_sum.192
  90.5 68.8 %all-gather.2.cloned.1.call-done = bf16[2,6400,128]{2,1,0:T(8,128)(2,1)} async-done(((bf16[2,400,128]{2,1,0:T(8,128)(2,1)}), bf16[2,6400,128]{2,1,0:T(8,128)(2,1)}) %all-gather.2.cloned.1.call-update) | async-done | bytes 3276816 | tf_op jit(solution)/shard_map/all_gather | solution.py:42
  159.3 1.4 fusion.142
  162.3 0.4 fusion.146
  162.7 0.4 fusion.147
  163.1 0.4 fusion.148
  163.4 0.4 fusion.149
  163.8 0.4 fusion.150
  164.2 0.4 fusion.151
  164.6 0.4 fusion.152
  168.5 0.4 fusion.53
  168.9 0.4 fusion.52
  169.3 0.4 fusion.51
  169.7 0.6 fusion.50
  170.3 0.4 fusion.49
  170.7 0.4 fusion.48
  171.1 0.4 fusion.47
  171.5 0.4 fusion.46
  171.9 0.4 fusion.45
  172.3 0.4 fusion.44
  172.7 0.4 fusion.43
  173.1 0.4 fusion.42
  173.8 0.6 copy.274
  174.4 0.5 broadcast.837
  174.9 1.8 reduce.42
  176.8 10.4 %all_to_all.24 = bf16[4,2,12288]{2,1,0:T(2,128)(2,1)S(1)} all-to-all(bf16[4,2,12288]{2,1,0:T(2,128)(2,1)S(1)} %reshape.2339), channel_id=1, replica_groups=mesh['grp'=2,'sp'=16,'tp'=4,'dp'=2] {'tp'}, dimensions={0} | all-to-all | bytes 393216 | tf_op jit(solution)/shard_map/all_to_all | solution.py:207
  188.0 3.8 %fusion.2 = bf16[1,96,2048]{2,1,0:T(8,128)(2,1)} fusion(bf16[1024,2048]{1,0:T(8,128)(2,1)} %param.31, bf16[1,96,2048]{2,1,0:T(8,128)(2,1)S(1)} %copy-done.1, f32[2048]{0:T(1024)S(1)} %bitcast.339, f32[96,1024]{1,0:T(8,128)S(1)} %bitcast.327, f32[1024]{0:T(1024)S(1)} %copy-done.9, f32[96]{0:T(128)S(1)} %add_rsqrt_fusion.2), kind=kOutput, calls=%fused_computation.3 | convolution fusion | flops 403734528 | bytes 5386624 | tf_op jit(solution)/shard_map/bsd,de->bse/dot_general | solution.py:209
  (93 shorter events, 9.3 us)
Async XLA Ops:
  6.5 0.9 copy-start
  6.6 55.8 %copy-start.1 = (bf16[1,96,2048]{2,1,0:T(8,128)(2,1)S(1)}, bf16[1,96,2048]{2,1,0:T(8,128)(2,1)}, u32[]{:S(2)}) copy-start(bf16[1,96,2048]{2,1,0:T(8,128)(2,1)} %param.16) | copy-start | bytes 1179652
  6.6 55.8 %copy-start.8 = (f32[2048]{0:T(1024)S(1)}, f32[2048]{0:T(1024)}, u32[]{:S(2)}) copy-start(f32[2048]{0:T(1024)} %param.23) | copy-start | bytes 24580
  11.3 40.2 %all-to-all-start = ((f32[16,3,2,512]{3,2,1,0:T(2,128)}), f32[16,3,2,512]{3,2,1,0:T(2,128)S(1)}, u32[]{:S(2)}, u32[]{:S(2)}) async-start(f32[16,3,2,512]{3,2,1,0:T(2,128)} %broadcast_in_dim.15), calls=%async_computation | async-start | bytes 393216 | tf_op jit(solution)/shard_map/all_to_all | solution.py:19
  52.2 10.1 %all-to-all-start.1 = ((f32[4,3,2,512]{3,2,1,0:T(2,128)}), f32[4,3,2,512]{3,2,1,0:T(2,128)S(1)}, u32[]{:S(2)}, u32[]{:S(2)}) async-start(f32[4,3,2,512]{3,2,1,0:T(2,128)} %broadcast_in_dim.16), calls=%async_computation.1 | async-start | bytes 98304 | tf_op jit(solution)/shard_map/all_to_all | solution.py:19
  63.9 3.9 %copy-start.10 = (f32[128]{0:T(128)S(1)}, f32[128]{0:T(128)}, u32[]{:S(2)}) copy-start(f32[128]{0:T(128)} %param.28) | copy-start | bytes 1540
  63.9 5.3 %copy-start.3 = (bf16[1,16,2048]{2,1,0:T(8,128)(2,1)S(1)}, bf16[1,16,2048]{2,1,0:T(8,128)(2,1)}, u32[]{:S(2)}) copy-start(bf16[1,16,2048]{2,1,0:T(8,128)(2,1)} %param.18) | copy-start | bytes 196612
  63.9 5.3 %copy-start.5 = (bf16[2048,128]{1,0:T(8,128)(2,1)S(1)}, bf16[2048,128]{1,0:T(8,128)(2,1)}, u32[]{:S(2)}) copy-start(bf16[2048,128]{1,0:T(8,128)(2,1)} %param.26) | copy-start | bytes 1572868
  63.9 5.6 %copy-start.4 = (bf16[2048,128]{1,0:T(8,128)(2,1)S(1)}, bf16[2048,128]{1,0:T(8,128)(2,1)}, u32[]{:S(2)}) copy-start(bf16[2048,128]{1,0:T(8,128)(2,1)} %param.25) | copy-start | bytes 1572868
  63.9 19.2 %all-to-all-start.2 = ((bf16[4,1,96,2048]{3,2,1,0:T(8,128)(2,1)}), bf16[4,1,96,2048]{3,2,1,0:T(8,128)(2,1)S(1)}, u32[]{:S(2)}, u32[]{:S(2)}) async-start(bf16[4,1,96,2048]{3,2,1,0:T(8,128)(2,1)} %broadcast_in_dim.19), calls=%async_computation.2 | async-start | bytes 3145728 | tf_op jit(solution)/shard_map/all_to_all | solution.py:19
  67.7 91.6 %all-gather.2.cloned.1.call-start = ((), (), s32[]{:S(2)}) async-start(), calls=%async_computation.4 | async-start | bytes 3481600 | tf_op jit(solution)/shard_map/all_gather | solution.py:42
  85.3 3.2 %copy-start.11 = (f32[128]{0:T(128)S(1)}, f32[128]{0:T(128)}, u32[]{:S(2)}) copy-start(f32[128]{0:T(128)} %param.27) | copy-start | bytes 1540
  85.3 3.4 %copy-start.6 = (f32[384,1,32]{0,2,1:T(8,128)S(1)}, f32[384,1,32]{0,2,1:T(8,128)}, u32[]{:S(2)}) copy-start(f32[384,1,32]{0,2,1:T(8,128)} %get-tuple-element.57) | copy-start | bytes 147460
  85.3 3.4 %copy-start.7 = (f32[384,1,32]{0,2,1:T(8,128)S(1)}, f32[384,1,32]{0,2,1:T(8,128)}, u32[]{:S(2)}) copy-start(f32[384,1,32]{0,2,1:T(8,128)} %get-tuple-element.72) | copy-start | bytes 147460
  85.3 3.7 %copy-start.12 = (f32[2]{0:T(128)S(1)}, f32[2]{0:T(128)}, u32[]{:S(2)}) copy-start(f32[2]{0:T(128)} %param.29) | copy-start | bytes 28
  159.3 2.0 %copy-start.2 = (bf16[2,6400,128]{2,1,0:T(8,128)(2,1)S(1)}, bf16[2,6400,128]{2,1,0:T(8,128)(2,1)}, u32[]{:S(2)}) copy-start(bf16[2,6400,128]{2,1,0:T(8,128)(2,1)} %all-gather.2.cloned.1.call-done) | copy-start | bytes 9830404
  187.2 0.8 copy-start.9
Sparse Core Ops, SparseCore 0:
  88.7 70.5 all-gather.1
where the time goes:
time: 199 us
  waiting for transfers between devices  102 us (51%)
  starting transfers between devices  32.4 us (16%)
  matrix products  20.7 us (10%)
  between operations  14 us (7%)
  other arithmetic  12.5 us (6%)
  blocking collectives  10.4 us (5%)
  local copies, waits for them, and re-layouts  7.17 us (4%)
    all_gather x1, waiting for transfers between devices, side_by_side(): lax.all_gather(both, axis, axis=dim, tiled=True)  68.8 us
    all_to_all x3, waiting for transfers between devices, copy_for_each(): lax.all_to_all(jnp.broadcast_to(x[None], (count, *x.shape)), axis, 0, 0,...  32.7 us
    all_to_all x3, starting transfers between devices, copy_for_each(): lax.all_to_all(jnp.broadcast_to(x[None], (count, *x.shape)), axis, 0, 0,...  32.4 us
    all_to_all x1, blocking collectives, on_device(): lax.all_to_all(attended, 'tp', split_axis=1, concat_axis=2, tiled=True)  10.4 us
    dot_general x13, matrix products, on_device(): jnp.einsum('bqkgd,bnkd->bkgqn', query_rows, key_heads, preferred_element_...  5.8 us
    dot_general x13, matrix products, on_device(): jnp.einsum('bkgqn,bnkd->bkgqd', exp_scores.astype(jnp.bfloat16), value_he...  5.21 us
  transfers between devices with their start and end apart: 4, of which 4 were waited for; matrix products, arithmetic and copies ran while one was open for 3% of the time, Pallas kernels for 0%

commit v1 on v0

v1 whole, which is shorter than its diff:
```python
import functools
import math

import jax
import jax.numpy as jnp
from jax import lax
from jax.experimental import pallas as pl
from jax.experimental.pallas import tpu as pltpu
from jax.sharding import PartitionSpec as P

HEADS = 8
KV_HEADS = 4
HEAD_DIM = 128
GRID_WIDTH = 64
EPSILON = 1e-06
LOG2E = math.log2(math.e)
MESH = pl.DeviceIdType.MESH
F32 = jnp.float32
BF16 = jnp.bfloat16
RELATIVE = (0, 3, 1, 2)


def kernel(
    n_sp,
    latent,
    cond,
    context,
    cond_ctx,
    w_shift,
    w_scale,
    w_gate,
    norm_gain,
    w_query,
    w_key,
    w_value,
    query_gain,
    key_gain,
    ctx_lift,
    out_gain,
    w_out,
    result,
    lat,
    ctx_rows,
    wm,
    wq,
    wkv,
    wo,
    part,
    got_mod,
    got_gate,
    own_mod,
    own_gate,
    mod_all,
    gate_all,
    rows_mod,
    normed,
    cos_t,
    sin_t,
    kv_r,
    kv_l,
    q_s,
    m_s,
    l_s,
    acc_s,
    att_send,
    att_all,
    att_n,
    out_v,
    loc,
    x_send,
    x_recv,
    chain,
    p1_send,
    p1_recv,
    g1_send,
    g1_recv,
    p2_send,
    p2_recv,
    g2_send,
    g2_recv,
    r_send,
    r_recv,
    o_send,
    o_recv,
):
    z = lax.axis_index("sp")
    x = lax.axis_index("tp")
    n_tp = 4
    tok = lat.shape[1]
    half = tok // 2
    n_ctx = ctx_rows.shape[0]
    seq = n_tp * tok
    rows = n_ctx + seq
    width = lat.shape[2]
    mate = z + 1 - 2 * lax.rem(z, 2)
    parity = lax.rem(z, 2)

    def sp(d):
        return lax.rem(z + d + n_sp, n_sp)

    def tp(d):
        return lax.rem(x + d + n_tp, n_tp)

    def remote(src, dst, s, r, **where):
        return pltpu.make_async_remote_copy(
            src_ref=src,
            dst_ref=dst,
            send_sem=s,
            recv_sem=r,
            device_id=where,
            device_id_type=MESH,
        )

    loads = [
        pltpu.make_async_copy(latent.at[0], lat.at[0], loc.at[0]),
        pltpu.make_async_copy(w_shift, wm.at[0], loc.at[1]),
        pltpu.make_async_copy(w_scale, wm.at[1], loc.at[2]),
        pltpu.make_async_copy(w_gate, wm.at[2], loc.at[3]),
        pltpu.make_async_copy(context.at[0], ctx_rows, loc.at[4]),
        pltpu.make_async_copy(w_key, wkv.at[:, pl.ds(0, HEAD_DIM)], loc.at[5]),
        pltpu.make_async_copy(w_value, wkv.at[:, pl.ds(HEAD_DIM, HEAD_DIM)], loc.at[6]),
        pltpu.make_async_copy(w_query, wq, loc.at[7]),
        pltpu.make_async_copy(w_out, wo, loc.at[8]),
    ]
    for copy in loads:
        copy.start()

    barrier = pltpu.get_barrier_semaphore()
    near = [dict(sp=sp(1)), dict(sp=sp(-1))]
    near += [dict(tp=tp(d)) for d in range(1, n_tp)]
    near += [dict(tp=tp(d), sp=mate) for d in range(1, n_tp)]
    for where in near:
        pl.semaphore_signal(barrier, inc=1, device_id=where, device_id_type=MESH)
    pl.semaphore_wait(barrier, len(near))

    lo, hi = pl.ds(0, half), pl.ds(half, half)
    x_copies = [
        remote(lat.at[0, lo], lat.at[1, lo], x_send.at[0], x_recv.at[0], tp=tp(1)),
        remote(lat.at[0, hi], lat.at[2, hi], x_send.at[1], x_recv.at[1], tp=tp(-1)),
        remote(lat.at[0, hi], lat.at[1, hi], x_send.at[2], x_recv.at[2], tp=tp(1)),
        remote(lat.at[0, lo], lat.at[2, lo], x_send.at[3], x_recv.at[3], tp=tp(-1)),
        remote(lat.at[1, lo], lat.at[3, lo], x_send.at[4], x_recv.at[4], tp=tp(1)),
        remote(lat.at[2, hi], lat.at[3, hi], x_send.at[5], x_recv.at[5], tp=tp(-1)),
    ]
    loads[0].wait()
    for copy in x_copies[:4]:
        copy.start()

    in_rows = wm.shape[1]
    lanes = pl.ds(pl.multiple_of(z * in_rows, in_rows), in_rows)
    own_in = cond[:, lanes].astype(F32)
    ctx_in = cond_ctx[:, lanes].astype(F32)
    first_row = lax.broadcasted_iota(jnp.int32, (16, in_rows), 0) == 0
    both = jnp.where(
        first_row,
        jnp.broadcast_to(own_in, (16, in_rows)),
        jnp.broadcast_to(ctx_in, (16, in_rows)),
    )
    activated = jax.nn.silu(both).astype(BF16)
    for kind in range(3):
        loads[1 + kind].wait()
        product = jnp.dot(activated, wm[kind], preferred_element_type=F32)
        if kind < 2:
            for who in range(2):
                for block in range(2):
                    for side in range(2):
                        at = (2 * block + side) * 128
                        row = (2 * kind + who) * 2 + side
                        part[block, row : row + 1, :] = product[who : who + 1, at : at + 128]
        else:
            part[2, :, :] = jnp.zeros((8, 128), F32)
            for side in range(4):
                part[2, side : side + 1, :] = product[0:1, side * 128 : side * 128 + 128]

    reach, turn = 1, 0
    while 2 * reach <= n_sp // 2:
        for d in (reach, -reach):
            pl.semaphore_signal(
                chain.at[turn], inc=1, device_id=dict(sp=sp(d)), device_id_type=MESH
            )
        pl.semaphore_wait(chain.at[turn], 2)
        reach, turn = 2 * reach, turn + 1

    def p1(d):
        to = lax.rem(z + d, n_sp)
        return remote(
            part.at[lax.rem(to, 2)],
            got_mod.at[d - 1],
            p1_send.at[d - 1],
            p1_recv.at[d - 1],
            sp=to,
        )

    def g1(d):
        to = lax.rem(z + d, n_sp)
        return remote(
            part.at[2], got_gate.at[d - 1], g1_send.at[d - 1], g1_recv.at[d - 1], sp=to
        )

    def each(start, stop, f):
        def body(i, carry):
            f(i)
            return carry

        lax.fori_loop(start, stop, body, 0)

    each(1, n_sp, lambda d: p1(d).start())
    each(1, n_sp, lambda d: g1(d).start())

    cos_t[0:n_ctx, :] = jnp.ones((n_ctx, HEAD_DIM), F32)
    sin_t[0:n_ctx, :] = jnp.zeros((n_ctx, HEAD_DIM), F32)
    lane = lax.broadcasted_iota(jnp.int32, (tok, HEAD_DIM), 1)
    place = lax.broadcasted_iota(jnp.int32, (tok, HEAD_DIM), 0)
    quarter = HEAD_DIM // 4
    inverse = jnp.exp((lane & (quarter - 1)).astype(F32) * (-math.log(10000.0) / quarter))
    lower = (lane & (2 * quarter - 1)) < quarter
    for j in range(n_tp):
        token = z * seq + tp(RELATIVE[j]) * tok + place
        grid_row = token >> (GRID_WIDTH.bit_length() - 1)
        grid_col = token & (GRID_WIDTH - 1)
        angle = jnp.where(lane < 2 * quarter, grid_row, grid_col).astype(F32) * inverse
        at = n_ctx + j * tok
        cos_t[at : at + tok, :] = jnp.cos(angle)
        sine = jnp.sin(angle)
        sin_t[at : at + tok, :] = jnp.where(lower, -sine, sine)

    x_copies[0].wait_recv()
    x_copies[4].start()
    x_copies[1].wait_recv()
    x_copies[5].start()

    each(1, n_sp, lambda d: p1(d).wait_recv())

    def add_up(own, got):
        return lax.fori_loop(0, n_sp - 1, lambda i, total: total + got[i], own)

    own_mod[...] = add_up(part[parity], got_mod)
    mod_all[x, parity] = own_mod[...]
    spread = [(d, e) for e in range(2) for d in range(n_tp) if (d, e) != (0, 0)]
    p2 = []
    for i, (d, e) in enumerate(spread):
        where = {}
        if d:
            where["tp"] = tp(d)
        if e:
            where["sp"] = mate
        p2.append(
            remote(own_mod, mod_all.at[x, parity], p2_send.at[i], p2_recv.at[i], **where)
        )
    for copy in p2:
        copy.start()
    each(1, n_sp, lambda d: g1(d).wait_recv())
    own_gate[...] = add_up(part[2], got_gate)
    gate_all[x] = own_gate[...]
    g2 = [
        remote(own_gate, gate_all.at[x], g2_send.at[d - 1], g2_recv.at[d - 1], tp=tp(d))
        for d in range(1, n_tp)
    ]
    for copy in g2:
        copy.start()

    for copy in loads[4:8]:
        copy.wait()
    for copy in p2:
        copy.wait_recv()

    cols = width // n_tp
    for b in range(n_tp):
        for block in range(2):
            tile = mod_all[b, block]
            for side in range(2):
                at = b * cols + (2 * block + side) * 128
                gain = norm_gain[:, at : at + 128]
                for who in range(2):
                    r = who * 2 + side
                    rows_mod[who : who + 1, at : at + 128] = tile[r : r + 1, :]
                    rows_mod[2 + who : 3 + who, at : at + 128] = gain * (
                        1.0 + tile[4 + r : 5 + r, :]
                    )

    def norm_rows(read, base, count, who):
        shift = rows_mod[who : who + 1, :]
        scale = rows_mod[2 + who : 3 + who, :]

        def body(i, carry):
            floats = read(pl.ds(pl.multiple_of(i * 16, 16), 16)).astype(F32)
            inv = lax.rsqrt(jnp.mean(floats * floats, -1, keepdims=True) + EPSILON)
            normed[pl.ds(pl.multiple_of(base + i * 16, 16), 16), :] = (
                floats * inv * scale + shift
            ).astype(BF16)
            return carry

        lax.fori_loop(0, count // 16, body, 0)

    def head_norm(raw, gain):
        floats = raw.astype(BF16).astype(F32)
        return floats * lax.rsqrt(jnp.mean(floats * floats, -1, keepdims=True) + EPSILON) * gain

    def rotate(vectors, at, count):
        d = lax.broadcasted_iota(jnp.int32, (count, HEAD_DIM), 1)
        swapped = jnp.where(
            (d & (2 * quarter - 1)) < quarter,
            pltpu.roll(vectors, HEAD_DIM - quarter, 1),
            pltpu.roll(vectors, quarter, 1),
        )
        return vectors * cos_t[at : at + count, :] + swapped * sin_t[at : at + count, :]

    bounds = [(0, n_ctx + tok)] + [(n_ctx + j * tok, tok) for j in range(1, n_tp)]

    def ring(way, slot, j):
        at, count = bounds[j]
        buf = kv_r if way == 0 else kv_l
        piece = pl.ds(at, count)
        target = sp(1) if way == 0 else sp(-1)
        return remote(
            buf.at[slot - 1, :, piece],
            buf.at[slot, :, piece],
            r_send.at[way, slot - 1, j],
            r_recv.at[way, slot - 1, j],
            sp=target,
        )

    norm_rows(lambda i: ctx_rows[i, :], 0, n_ctx, 1)
    for j in range(n_tp):
        if j == 1:
            x_copies[2].wait_recv()
        if j == 2:
            x_copies[3].wait_recv()
        if j == 3:
            x_copies[4].wait_recv()
            x_copies[5].wait_recv()
        norm_rows(lambda i, j=j: lat[j, i, :], n_ctx + j * tok, tok, 0)
        at, count = bounds[j]
        made = jnp.dot(normed[at : at + count, :], wkv[...], preferred_element_type=F32)
        keys = rotate(head_norm(made[:, :HEAD_DIM], key_gain[...]), at, count).astype(BF16)
        values = made[:, HEAD_DIM:].astype(BF16)
        kv_r[0, 0, at : at + count, :] = keys
        kv_l[0, 0, at : at + count, :] = keys
        kv_r[0, 1, at : at + count, :] = values
        kv_l[0, 1, at : at + count, :] = values
        ring(0, 1, j).start()
        ring(1, 1, j).start()

    made = jnp.dot(normed[n_ctx:rows, :], wq[...], preferred_element_type=F32)
    for g in range(2):
        q_s[g] = rotate(
            head_norm(made[:, g * HEAD_DIM : (g + 1) * HEAD_DIM], query_gain[...]), n_ctx, seq
        ).astype(BF16)

    last = n_sp // 2
    factor = LOG2E * HEAD_DIM ** (-0.5)
    nt = (((1,), (1,)), ((), ()))

    def attend(g, keys, values, first=False, lift_from=None):
        scores = lax.dot_general(q_s[g], keys, nt, preferred_element_type=F32) * factor
        if lift_from is not None:
            lift = (ctx_lift[g] + math.log(seq / n_ctx)) * LOG2E
            at = lax.broadcasted_iota(jnp.int32, (1, keys.shape[0]), 1)
            scores = scores + jnp.where(at >= lift_from, lift, 0.0)
        top = jnp.max(scores, -1, keepdims=True)
        if not first:
            before = m_s[g]
            top = jnp.maximum(before, top)
        weights = jnp.exp2(scores - top)
        total = jnp.sum(weights, -1, keepdims=True)
        out = jnp.dot(weights.astype(BF16), values, preferred_element_type=F32)
        if not first:
            keep = jnp.exp2(before - top)
            total = total + l_s[g] * keep
            out = out + acc_s[g] * keep
        m_s[g] = top
        l_s[g] = total
        acc_s[g] = out

    def pull(s, j):
        for way in range(2):
            short = (j < 2) if way == 0 else (j >= 2)

            def wait(way=way):
                ring(way, s, j).wait_recv()

            def forward(way=way):
                ring(way, s + 1, j).start()

            if short:
                wait()
                pl.when(s < last)(forward)
            else:
                pl.when(s < last)(wait)
                pl.when(s < last - 1)(forward)

    body_rows = pl.ds(n_ctx, seq)
    for j in range(2):
        pull(1, j)
    attend(0, kv_r[0, 0, body_rows], kv_r[0, 1, body_rows], first=True)
    for j in range(2, 4):
        pull(1, j)
    attend(1, kv_r[0, 0, body_rows], kv_r[0, 1, body_rows], first=True)

    def step(s, carry):
        for g in range(2):
            for j in (2 * g, 2 * g + 1):
                pull(s, j)
            keys = jnp.concatenate([kv_r[s - 1, 0, body_rows], kv_l[s - 1, 0, body_rows]], 0)
            values = jnp.concatenate([kv_r[s - 1, 1, body_rows], kv_l[s - 1, 1, body_rows]], 0)
            attend(g, keys, values)
        return carry

    lax.fori_loop(2, last + 1, step, 0)

    def ending(kind):
        at, count = bounds[2]
        parts = [kv_r[last, kind, n_ctx:at], kv_l[last, kind, at:rows]]
        parts += [kv_r[s, kind, 0:n_ctx] for s in range(last + 1)]
        parts += [kv_l[s, kind, 0:n_ctx] for s in range(1, last)]
        return jnp.concatenate(parts, 0)

    end_keys = ending(0)
    end_values = ending(1)
    for g in range(2):
        attend(g, end_keys, end_values, lift_from=seq)
        att = (acc_s[g] / l_s[g]).astype(BF16)
        for j in range(n_tp):
            att_send[j, :, g * HEAD_DIM : (g + 1) * HEAD_DIM] = att[j * tok : (j + 1) * tok]

    exchange = [
        remote(
            att_send.at[j], att_all.at[x], o_send.at[j - 1], o_recv.at[j - 1], tp=tp(RELATIVE[j])
        )
        for j in range(1, n_tp)
    ]
    for copy in exchange:
        copy.start()
    att_all[x] = att_send[0]
    for copy in g2:
        copy.wait_recv()
    for b in range(n_tp):
        for side in range(4):
            at = b * cols + side * 128
            rows_mod[4:5, at : at + 128] = gate_all[b, side : side + 1, :]
    loads[8].wait()
    for copy in exchange:
        copy.wait_recv()

    channels = att_all.shape[2]
    pieces = [att_all[b].astype(F32) for b in range(n_tp)]
    square = sum(jnp.sum(p * p, -1, keepdims=True) for p in pieces)
    inv = lax.rsqrt(square * (1.0 / (n_tp * channels)) + EPSILON)
    for b in range(n_tp):
        gain = out_gain[:, b * channels : (b + 1) * channels]
        att_n[:, b * channels : (b + 1) * channels] = (pieces[b] * inv * gain).astype(BF16)
    strip = 512
    stores = []
    for i in range(width // strip):
        at = pl.ds(i * strip, strip)
        mix = jnp.dot(att_n[...], wo[:, at], preferred_element_type=F32)
        out_v[:, at] = (lat[0, :, at].astype(F32) + rows_mod[4:5, at] * mix).astype(BF16)
        store = pltpu.make_async_copy(out_v.at[:, at], result.at[0, :, at], loc.at[9 + i])
        store.start()
        stores.append(store)

    for copy in x_copies + p2 + g2 + exchange:
        copy.wait_send()
    each(1, n_sp, lambda d: p1(d).wait_send())
    each(1, n_sp, lambda d: g1(d).wait_send())

    def drain(s, carry):
        for j in range(4):
            for way in range(2):
                short = (j < 2) if way == 0 else (j >= 2)

                def wait(way=way, j=j):
                    ring(way, s, j).wait_send()

                if short:
                    wait()
                else:
                    pl.when(s < last)(wait)
        return carry

    lax.fori_loop(1, last + 1, drain, 0)
    for store in stores:
        store.wait()


def on_device(mesh, *args):
    (
        latent,
        cond,
        context,
        cond_ctx,
        w_shift,
        w_scale,
        w_gate,
        norm_gain,
        w_query,
        w_key,
        w_value,
        query_gain,
        key_gain,
        ctx_lift,
        out_gain,
        w_out,
    ) = args
    n_sp, n_tp = mesh.shape["sp"], mesh.shape["tp"]
    assert n_tp == 4 and KV_HEADS == n_tp and n_sp % 4 == 0
    tok, width = latent.shape[1:]
    n_ctx = context.shape[1]
    rows = n_ctx + n_tp * tok
    seq = n_tp * tok
    slots = n_sp // 2 + 1
    any_ = pl.BlockSpec(memory_space=pl.ANY)
    vmem = pl.BlockSpec(memory_space=pltpu.VMEM)
    smem = pl.BlockSpec(memory_space=pltpu.SMEM)
    dma = pltpu.SemaphoreType.DMA
    scratch = [
        pltpu.VMEM((n_tp, tok, width), BF16),
        pltpu.VMEM((n_ctx, width), BF16),
        pltpu.VMEM((3,) + w_shift.shape, BF16),
        pltpu.VMEM(w_query.shape, BF16),
        pltpu.VMEM((width, 2 * HEAD_DIM), BF16),
        pltpu.VMEM(w_out.shape, BF16),
        pltpu.VMEM((3, 8, 128), F32),
        pltpu.VMEM((n_sp - 1, 8, 128), F32),
        pltpu.VMEM((n_sp - 1, 8, 128), F32),
        pltpu.VMEM((8, 128), F32),
        pltpu.VMEM((8, 128), F32),
        pltpu.VMEM((n_tp, 2, 8, 128), F32),
        pltpu.VMEM((n_tp, 8, 128), F32),
        pltpu.VMEM((8, width), F32),
        pltpu.VMEM((rows, width), BF16),
        pltpu.VMEM((rows, HEAD_DIM), F32),
        pltpu.VMEM((rows, HEAD_DIM), F32),
        pltpu.VMEM((slots, 2, rows, HEAD_DIM), BF16),
        pltpu.VMEM((slots, 2, rows, HEAD_DIM), BF16),
        pltpu.VMEM((2, seq, HEAD_DIM), BF16),
        pltpu.VMEM((2, seq, 1), F32),
        pltpu.VMEM((2, seq, 1), F32),
        pltpu.VMEM((2, seq, HEAD_DIM), F32),
        pltpu.VMEM((n_tp, tok, 2 * HEAD_DIM), BF16),
        pltpu.VMEM((n_tp, tok, 2 * HEAD_DIM), BF16),
        pltpu.VMEM((tok, HEADS * HEAD_DIM), BF16),
        pltpu.VMEM((tok, width), BF16),
        dma((13,)),
        dma((6,)),
        dma((6,)),
        pltpu.SemaphoreType.REGULAR((3,)),
        dma((n_sp - 1,)),
        dma((n_sp - 1,)),
        dma((n_sp - 1,)),
        dma((n_sp - 1,)),
        dma((7,)),
        dma((7,)),
        dma((3,)),
        dma((3,)),
        dma((2, slots - 1, 4)),
        dma((2, slots - 1, 4)),
        dma((3,)),
        dma((3,)),
    ]
    specs = [any_, vmem, any_, vmem, any_, any_, any_, vmem]
    specs += [any_, any_, any_, vmem, vmem, smem, vmem, any_]
    row = lambda a: a.reshape(1, -1)
    return pl.pallas_call(
        functools.partial(kernel, n_sp),
        out_shape=jax.ShapeDtypeStruct(latent.shape, BF16),
        in_specs=specs,
        out_specs=any_,
        scratch_shapes=scratch,
        compiler_params=pltpu.CompilerParams(
            collective_id=0, has_side_effects=True, vmem_limit_bytes=56 << 20
        ),
    )(
        latent,
        cond,
        context,
        row(cond_ctx),
        w_shift,
        w_scale,
        w_gate,
        row(norm_gain),
        w_query,
        w_key,
        w_value,
        row(query_gain),
        row(key_gain),
        ctx_lift,
        row(out_gain),
        w_out,
    )


def solution(mesh):
    in_specs = (
        P(("grp", "dp"), ("sp", "tp"), None),
        P(("grp", "dp"), None),
        P(("grp", "dp"), "sp", None),
        P(),
        P("sp", "tp"),
        P("sp", "tp"),
        P("sp", "tp"),
        P(),
        P(None, "tp"),
        P(None, "tp"),
        P(None, "tp"),
        P(),
        P(),
        P("tp"),
        P(),
        P(),
    )
    out_specs = P(("grp", "dp"), ("sp", "tp"), None)
    return jax.shard_map(
        functools.partial(on_device, mesh),
        mesh=mesh,
        in_specs=in_specs,
        out_specs=out_specs,
        check_vma=False,
    )
```

time: 199 us -> 96.1 us (0.48)
  waiting for transfers between devices: 102 us -> 0 us
  Pallas kernels: 0 us -> 92.8 us
  starting transfers between devices: 32.4 us -> 0 us
  matrix products: 20.7 us -> 0 us
  between operations: 14 us -> 0.01 us
  other arithmetic: 12.5 us -> 0 us
  blocking collectives: 10.4 us -> 0 us
  local copies, waits for them, and re-layouts: 7.17 us -> 3.06 us
    pallas_call x0 -> x1, Pallas kernels: none -> 92.8 us  [on_device(): pl.pallas_call(functools.partial(kernel, n_sp), out_shape=jax.ShapeDtypeS...]
    all_gather x1 -> x0, waiting for transfers between devices: 68.8 us -> none  [side_by_side(): lax.all_gather(both, axis, axis=dim, tiled=True)]
    all_to_all x3 -> x0, waiting for transfers between devices: 32.7 us -> none  [copy_for_each(): lax.all_to_all(jnp.broadcast_to(x[None], (count, *x.shape)), axis, 0, 0,...]
    all_to_all x3 -> x0, starting transfers between devices: 32.4 us -> none  [copy_for_each(): lax.all_to_all(jnp.broadcast_to(x[None], (count, *x.shape)), axis, 0, 0,...]
    dot_general x33 -> x0, matrix products: 20.7 us -> none  [the longest x13 5.8 us: on_device(): jnp.einsum('bqkgd,bnkd->bkgqn', query_rows, key_heads, preferred_element_...]
    all_to_all x1 -> x0, blocking collectives: 10.4 us -> none  [on_device(): lax.all_to_all(attended, 'tp', split_axis=1, concat_axis=2, tiled=True)]
    reduce_sum x20 -> x0, other arithmetic: 5.89 us -> none  [the longest x13 2.88 us: on_device(): running_sum = running_sum * keep_factor + jnp.sum(exp_scores, -1)]
    broadcast_in_dim x4 -> x0, local copies, waits for them, and re-layouts: 3.46 us -> none  [the longest x3 2.7 us: copy_for_each(): jnp.broadcast_to(x[None], (count, *x.shape))]
  transfers between devices with their start and end apart: 4 -> 0, of which waited for: 4 -> 0; matrix products, arithmetic and copies ran while one was open for 3% -> 0% of each run, Pallas kernels for 0% -> 0%
where the time goes in v1:
time: 96.1 us; the launch traced here: 95.9 us
  Pallas kernels  92.8 us (97%)
  local copies, waits for them, and re-layouts  3.06 us (3%)
    pallas_call x1, Pallas kernels, on_device(): pl.pallas_call(functools.partial(kernel, n_sp), out_shape=jax.ShapeDtypeS...  92.8 us

profile of v1, /device:TPU:40, one launch (start us, length us, event | category | flops | bytes accessed | tf_op | source)
XLA Modules:
  0.0 95.9 jit_solution(15771260643681970484)
XLA Ops:
  0.0 1.3 %reshape.15.cond_ctx = bf16[1,2048]{1,0:T(2,128)(2,1)} reshape(bf16[2048]{0:T(1024)(128)(2,1)} %param.19) | data formatting | bytes 8192 | tf_op jit(solution)/shard_map/reshape | solution.py:563
  1.3 92.8 %shard_map.154 = bf16[1,96,2048]{2,1,0:T(8,128)(2,1)} custom-call(bf16[1,96,2048]{2,1,0:T(8,128)(2,1)} %latent.1, bf16[1,2048]{1,0:T(2,128)(2,1)} %cond.1, bf16[1,16,2048]{2,1,0:T(8,128)(2,1)} %context.1, bf16[1,2048]{1,0:T(2,128)(2,1)} %reshape.15.cond_ctx, bf16[128,512]{1,0:T(8,128)(2,1)} %w_shift.1, bf16[128,512]{1,0:T(8,128)(2,1)} %w_scale.1, ...), custom_call_target="tpu_custom_call" | custom-call | tf_op jit(solution)/shard_map/pallas_call | solution.py:564
  94.1 1.8 %copy.18 = bf16[1,96,2048]{2,1,0:T(8,128)(2,1)} copy(bf16[1,96,2048]{2,1,0:T(8,128)(2,1)} %shard_map.154) | data formatting | bytes 786432

commit v2 on v1

v2 whole, which is shorter than its diff:
```python
import functools
import math

import jax
import jax.numpy as jnp
from jax import lax
from jax.experimental import pallas as pl
from jax.experimental.pallas import tpu as pltpu
from jax.sharding import PartitionSpec as P

HEADS = 8
KV_HEADS = 4
HEAD_DIM = 128
GRID_WIDTH = 64
EPSILON = 1e-06
LOG2E = math.log2(math.e)
MESH = pl.DeviceIdType.MESH
F32 = jnp.float32
BF16 = jnp.bfloat16
RELATIVE = (0, 3, 1, 2)


def kernel(
    n_sp,
    latent,
    cond_h,
    context,
    cond_ctx_h,
    w_shift,
    w_scale,
    w_gate,
    norm_gain_h,
    w_query,
    w_key,
    w_value,
    query_gain_h,
    key_gain_h,
    ctx_lift,
    out_gain_h,
    w_out,
    result,
    cond,
    cond_ctx,
    norm_gain,
    query_gain,
    key_gain,
    out_gain,
    lat,
    ctx_rows,
    wm,
    wq,
    wkv,
    wo,
    part,
    got_mod,
    own_mod,
    mod_all,
    rows_mod,
    unit,
    normed,
    cos_t,
    sin_t,
    kv_r,
    kv_l,
    q_s,
    m_s,
    l_s,
    acc_s,
    att_send,
    att_all,
    att_n,
    out_v,
    loc,
    x_send,
    x_recv,
    p1_send,
    p1_recv,
    p2_send,
    p2_recv,
    r_send,
    r_recv,
    o_send,
    o_recv,
):
    z = lax.axis_index("sp")
    x = lax.axis_index("tp")
    n_tp = 4
    tok = lat.shape[1]
    half = tok // 2
    n_ctx = ctx_rows.shape[0]
    seq = n_tp * tok
    rows = n_ctx + seq
    width = lat.shape[2]
    mate = z + 1 - 2 * lax.rem(z, 2)
    parity = lax.rem(z, 2)

    def sp(d):
        return lax.rem(z + d + n_sp, n_sp)

    def tp(d):
        return lax.rem(x + d + n_tp, n_tp)

    def remote(src, dst, s, r, **where):
        return pltpu.make_async_remote_copy(
            src_ref=src,
            dst_ref=dst,
            send_sem=s,
            recv_sem=r,
            device_id=where,
            device_id_type=MESH,
        )

    def each(start, stop, f):
        def body(i, carry):
            f(i)
            return carry

        lax.fori_loop(start, stop, body, 0)

    barrier = pltpu.get_barrier_semaphore()

    def greet(**where):
        pl.semaphore_signal(barrier, inc=1, device_id=where, device_id_type=MESH)

    for d in range(1, n_tp):
        greet(tp=tp(d))
        greet(tp=tp(d), sp=mate)
    each(1, n_sp, lambda d: greet(sp=lax.rem(z + d, n_sp)))

    def load(src, dst, i):
        copy = pltpu.make_async_copy(src, dst, loc.at[i])
        copy.start()
        return copy

    load_cond = load(cond_h, cond, 0)
    load_cond_ctx = load(cond_ctx_h, cond_ctx, 1)
    for kind, matrix in enumerate((w_shift, w_scale, w_gate)):
        load(matrix, wm.at[kind], 2)
    load_lat = load(latent.at[0], lat.at[0], 3)
    load_ctx = load(context.at[0], ctx_rows, 4)
    load(w_key, wkv.at[:, pl.ds(0, HEAD_DIM)], 5)
    load(w_value, wkv.at[:, pl.ds(HEAD_DIM, HEAD_DIM)], 5)
    load_gain = load(norm_gain_h, norm_gain, 6)
    load_key_gain = load(key_gain_h, key_gain, 7)
    load_wq = load(w_query, wq, 8)
    load_query_gain = load(query_gain_h, query_gain, 9)
    load_wo = load(w_out, wo, 10)
    load_out_gain = load(out_gain_h, out_gain, 11)

    def arrived(whole, i):
        pltpu.make_async_copy(whole, whole, loc.at[i]).wait()

    in_rows = wm.shape[1]
    load_cond.wait()
    load_cond_ctx.wait()
    lanes = pl.ds(pl.multiple_of(z * in_rows, in_rows), in_rows)
    own_in = cond[:, lanes].astype(F32)
    every = cond_ctx[...].astype(F32)
    line = lax.broadcasted_iota(jnp.int32, every.shape, 0)
    ctx_in = jnp.sum(jnp.where(line == z, every, 0.0), 0, keepdims=True)
    first_row = lax.broadcasted_iota(jnp.int32, (16, in_rows), 0) == 0
    both = jnp.where(
        first_row,
        jnp.broadcast_to(own_in, (16, in_rows)),
        jnp.broadcast_to(ctx_in, (16, in_rows)),
    )
    activated = jax.nn.silu(both).astype(BF16)
    arrived(wm, 2)
    for kind in range(3):
        product = jnp.dot(activated, wm[kind], preferred_element_type=F32)
        for who in range(2 if kind < 2 else 1):
            for block in range(2):
                for side in range(2):
                    at = (2 * block + side) * 128
                    row = (2 * kind + who) * 2 + side
                    part[block, row : row + 1, :] = product[who : who + 1, at : at + 128]

    load_lat.wait()
    pl.semaphore_wait(barrier, n_sp - 1 + 2 * (n_tp - 1))

    used = pl.ds(0, 10)

    def p1(d):
        to = lax.rem(z + d, n_sp)
        return remote(
            part.at[lax.rem(to, 2), used],
            got_mod.at[d - 1, used],
            p1_send.at[0],
            p1_recv.at[0],
            sp=to,
        )

    each(1, n_sp, lambda d: p1(d).start())

    lo, hi = pl.ds(0, half), pl.ds(half, half)
    x_copies = [
        remote(lat.at[0, lo], lat.at[1, lo], x_send.at[0], x_recv.at[0], tp=tp(1)),
        remote(lat.at[0, hi], lat.at[2, hi], x_send.at[0], x_recv.at[1], tp=tp(-1)),
        remote(lat.at[0, hi], lat.at[1, hi], x_send.at[0], x_recv.at[2], tp=tp(1)),
        remote(lat.at[0, lo], lat.at[2, lo], x_send.at[0], x_recv.at[3], tp=tp(-1)),
        remote(lat.at[1, lo], lat.at[3, lo], x_send.at[0], x_recv.at[4], tp=tp(1)),
        remote(lat.at[2, hi], lat.at[3, hi], x_send.at[0], x_recv.at[4], tp=tp(-1)),
    ]
    for copy in x_copies[:4]:
        copy.start()

    cos_t[0:n_ctx, :] = jnp.ones((n_ctx, HEAD_DIM), F32)
    sin_t[0:n_ctx, :] = jnp.zeros((n_ctx, HEAD_DIM), F32)
    lane = lax.broadcasted_iota(jnp.int32, (tok, HEAD_DIM), 1)
    place = lax.broadcasted_iota(jnp.int32, (tok, HEAD_DIM), 0)
    quarter = HEAD_DIM // 4
    inverse = jnp.exp((lane & (quarter - 1)).astype(F32) * (-math.log(10000.0) / quarter))
    lower = (lane & (2 * quarter - 1)) < quarter
    for j in range(n_tp):
        token = z * seq + tp(RELATIVE[j]) * tok + place
        grid_row = token >> (GRID_WIDTH.bit_length() - 1)
        grid_col = token & (GRID_WIDTH - 1)
        angle = jnp.where(lane < 2 * quarter, grid_row, grid_col).astype(F32) * inverse
        at = n_ctx + j * tok
        cos_t[at : at + tok, :] = jnp.cos(angle)
        sine = jnp.sin(angle)
        sin_t[at : at + tok, :] = jnp.where(lower, -sine, sine)

    def prepare(read, base, count):
        def body(i, carry):
            floats = read(pl.ds(pl.multiple_of(i * 16, 16), 16)).astype(F32)
            inv = lax.rsqrt(jnp.mean(floats * floats, -1, keepdims=True) + EPSILON)
            unit[pl.ds(pl.multiple_of(base + i * 16, 16), 16), :] = floats * inv
            return carry

        lax.fori_loop(0, count // 16, body, 0)

    load_ctx.wait()
    prepare(lambda i: ctx_rows[i, :], 0, n_ctx)
    prepare(lambda i: lat[0, i, :], n_ctx, tok)
    arrived(wkv, 5)
    load_gain.wait()
    load_key_gain.wait()

    every_got = got_mod.at[:, used]
    remote(every_got, every_got, p1_send.at[0], p1_recv.at[0], sp=mate).wait_recv()
    own_mod[...] = lax.fori_loop(
        0, n_sp - 1, lambda i, total: total + got_mod[i, 0:10, :], part[parity, 0:10, :]
    )
    mod_all[x, parity, 0:10, :] = own_mod[...]
    spread = [(d, e) for e in (1, 0) for d in (2, 1, 3, 0) if (d, e) != (0, 0)]
    p2 = []
    for i, (d, e) in enumerate(spread):
        where = {}
        if d:
            where["tp"] = tp(d)
        if e:
            where["sp"] = mate
        p2.append(
            remote(own_mod, mod_all.at[x, parity, used], p2_send.at[0], p2_recv.at[i], **where)
        )
    for copy in p2:
        copy.start()

    x_copies[0].wait_recv()
    x_copies[4].start()
    x_copies[1].wait_recv()
    x_copies[5].start()
    x_copies[2].wait_recv()
    prepare(lambda i: lat[1, i, :], n_ctx + tok, tok)
    x_copies[3].wait_recv()
    prepare(lambda i: lat[2, i, :], n_ctx + 2 * tok, tok)
    for copy in p2:
        copy.wait_recv()

    cols = width // n_tp
    for b in range(n_tp):
        for block in range(2):
            tile = mod_all[b, block, 0:10, :]
            for side in range(2):
                at = b * cols + (2 * block + side) * 128
                gain = norm_gain[:, at : at + 128]
                for who in range(2):
                    r = who * 2 + side
                    rows_mod[who : who + 1, at : at + 128] = tile[r : r + 1, :]
                    rows_mod[2 + who : 3 + who, at : at + 128] = gain * (
                        1.0 + tile[4 + r : 5 + r, :]
                    )
                rows_mod[4:5, at : at + 128] = tile[8 + side : 9 + side, :]

    def norm_rows(base, count, who):
        shift = rows_mod[who : who + 1, :]
        scale = rows_mod[2 + who : 3 + who, :]

        def body(i, carry):
            at = pl.ds(pl.multiple_of(base + i * 16, 16), 16)
            normed[at, :] = (unit[at, :] * scale + shift).astype(BF16)
            return carry

        lax.fori_loop(0, count // 16, body, 0)

    def head_norm(raw, gain):
        floats = raw.astype(BF16).astype(F32)
        return floats * lax.rsqrt(jnp.mean(floats * floats, -1, keepdims=True) + EPSILON) * gain

    def rotate(vectors, at, count):
        d = lax.broadcasted_iota(jnp.int32, (count, HEAD_DIM), 1)
        swapped = jnp.where(
            (d & (2 * quarter - 1)) < quarter,
            pltpu.roll(vectors, HEAD_DIM - quarter, 1),
            pltpu.roll(vectors, quarter, 1),
        )
        return vectors * cos_t[at : at + count, :] + swapped * sin_t[at : at + count, :]

    bounds = [(0, n_ctx + tok)] + [(n_ctx + j * tok, tok) for j in range(1, n_tp)]

    def ring(way, slot, j, final=False):
        at, count = bounds[j]
        buf = kv_r if way == 0 else kv_l
        piece = pl.ds(at, count)
        target = sp(1) if way == 0 else sp(-1)
        return remote(
            buf.at[slot - 1, :, piece],
            buf.at[slot, :, piece],
            r_send.at[way + 2 if final else way],
            r_recv.at[way, slot - 1, j],
            sp=target,
        )

    norm_rows(0, n_ctx, 1)
    for j in range(n_tp):
        at, count = bounds[j]
        if j == 3:
            remote(lat.at[3], lat.at[3], x_send.at[0], x_recv.at[4], tp=tp(1)).wait_recv()
            prepare(lambda i: lat[3, i, :], n_ctx + 3 * tok, tok)
        norm_rows(n_ctx + j * tok, tok, 0)
        made = jnp.dot(normed[at : at + count, :], wkv[...], preferred_element_type=F32)
        keys = rotate(head_norm(made[:, :HEAD_DIM], key_gain[...]), at, count).astype(BF16)
        values = made[:, HEAD_DIM:].astype(BF16)
        kv_r[0, 0, at : at + count, :] = keys
        kv_l[0, 0, at : at + count, :] = keys
        kv_r[0, 1, at : at + count, :] = values
        kv_l[0, 1, at : at + count, :] = values
        ring(0, 1, j).start()
        ring(1, 1, j).start()

    last = n_sp // 2
    factor = LOG2E * HEAD_DIM ** (-0.5)
    nt = (((1,), (1,)), ((), ()))

    def attend(g, keys, values, first=False, lift_from=None):
        scores = lax.dot_general(q_s[g], keys, nt, preferred_element_type=F32) * factor
        if lift_from is not None:
            lift = (ctx_lift[g] + math.log(seq / n_ctx)) * LOG2E
            at = lax.broadcasted_iota(jnp.int32, (1, keys.shape[0]), 1)
            scores = scores + jnp.where(at >= lift_from, lift, 0.0)
        top = jnp.max(scores, -1, keepdims=True)
        if not first:
            before = m_s[g]
            top = jnp.maximum(before, top)
        weights = jnp.exp2(scores - top)
        total = jnp.sum(weights, -1, keepdims=True)
        out = jnp.dot(weights.astype(BF16), values, preferred_element_type=F32)
        if not first:
            keep = jnp.exp2(before - top)
            total = total + l_s[g] * keep
            out = out + acc_s[g] * keep
        m_s[g] = top
        l_s[g] = total
        acc_s[g] = out

    def pull(s, j):
        for way in range(2):
            short = (j < 2) if way == 0 else (j >= 2)

            def wait(way=way):
                ring(way, s, j).wait_recv()

            def forward(final, way=way):
                ring(way, s + 1, j, final).start()

            if isinstance(s, int):
                if s < last or short:
                    wait()
                if s + 1 < last:
                    forward(False)
                elif s + 1 == last and short:
                    forward(True)
                continue
            wait()
            pl.when(s + 1 < last)(functools.partial(forward, False))
            if short:
                pl.when(s + 1 == last)(functools.partial(forward, True))

    body_rows = pl.ds(n_ctx, seq)
    pull(1, 0)
    load_wq.wait()
    load_query_gain.wait()
    made = jnp.dot(normed[n_ctx:rows, :], wq[...], preferred_element_type=F32)
    for g in range(2):
        q_s[g] = rotate(
            head_norm(made[:, g * HEAD_DIM : (g + 1) * HEAD_DIM], query_gain[...]), n_ctx, seq
        ).astype(BF16)
    pull(1, 1)
    attend(0, kv_r[0, 0, body_rows], kv_r[0, 1, body_rows], first=True)
    pull(1, 2)
    pull(1, 3)
    attend(1, kv_r[0, 0, body_rows], kv_r[0, 1, body_rows], first=True)

    def pair(slot, kind):
        return jnp.concatenate([kv_r[slot, kind, body_rows], kv_l[slot, kind, body_rows]], 0)

    def step(s, carry):
        for g in range(2):
            for j in (2 * g, 2 * g + 1):
                pull(s, j)
            attend(g, pair(s - 1, 0), pair(s - 1, 1))
        return carry

    lax.fori_loop(2, last, step, 0)
    for g in range(2):
        attend(g, pair(last - 1, 0), pair(last - 1, 1))

    def chunk(way, kind, j):
        at = n_ctx + j * tok
        return (kv_r if way == 0 else kv_l)[last, kind, at : at + tok]

    def ending(kind):
        parts = [chunk(0, kind, 0), chunk(1, kind, 2)]
        parts += [kv_r[s, kind, 0:n_ctx] for s in range(last + 1)]
        parts += [kv_l[s, kind, 0:n_ctx] for s in range(1, last)]
        return jnp.concatenate(parts, 0)

    pull(last, 0)
    pull(last, 2)
    for g in range(2):
        attend(g, ending(0), ending(1), lift_from=2 * tok)
    pull(last, 1)
    pull(last, 3)

    def exchange(g, j):
        part_of = pl.ds(g * HEAD_DIM, HEAD_DIM)
        return remote(
            att_send.at[j, :, part_of],
            att_all.at[x, :, part_of],
            o_send.at[0],
            o_recv.at[j - 1],
            tp=tp(RELATIVE[j]),
        )

    for g in range(2):
        attend(
            g,
            jnp.concatenate([chunk(0, 0, 1), chunk(1, 0, 3)], 0),
            jnp.concatenate([chunk(0, 1, 1), chunk(1, 1, 3)], 0),
        )
        att = (acc_s[g] / l_s[g]).astype(BF16)
        for j in range(n_tp):
            att_send[j, :, g * HEAD_DIM : (g + 1) * HEAD_DIM] = att[j * tok : (j + 1) * tok]
        for j in (3, 1, 2):
            exchange(g, j).start()
    att_all[x] = att_send[0]
    load_wo.wait()
    load_out_gain.wait()
    for j in range(1, n_tp):
        whole = att_all.at[tp(-RELATIVE[j])]
        remote(whole, whole, o_send.at[0], o_recv.at[j - 1], tp=tp(1)).wait_recv()

    channels = att_all.shape[2]
    pieces = [att_all[b].astype(F32) for b in range(n_tp)]
    square = sum(jnp.sum(p * p, -1, keepdims=True) for p in pieces)
    inv = lax.rsqrt(square * (1.0 / (n_tp * channels)) + EPSILON)
    for b in range(n_tp):
        gain = out_gain[:, b * channels : (b + 1) * channels]
        att_n[:, b * channels : (b + 1) * channels] = (pieces[b] * inv * gain).astype(BF16)
    strip = 512
    for i in range(width // strip):
        at = pl.ds(i * strip, strip)
        mix = jnp.dot(att_n[...], wo[:, at], preferred_element_type=F32)
        out_v[:, at] = (lat[0, :, at].astype(F32) + rows_mod[4:5, at] * mix).astype(BF16)
        pltpu.make_async_copy(out_v.at[:, at], result.at[0, :, at], loc.at[12]).start()

    def sent(whole, sem):
        remote(whole, whole, sem, p1_recv.at[0], sp=mate).wait_send()

    sent(lat.at[0:3], x_send.at[0])
    sent(every_got, p1_send.at[0])
    sent(got_mod.at[0 : len(p2), used], p2_send.at[0])
    sent(kv_r.at[0 : last - 1], r_send.at[0])
    sent(kv_l.at[0 : last - 1], r_send.at[1])
    at, _ = bounds[2]
    sent(kv_r.at[last - 1, :, 0:at], r_send.at[2])
    sent(kv_l.at[last - 1, :, at:rows], r_send.at[3])
    sent(att_send.at[1:n_tp], o_send.at[0])
    pltpu.make_async_copy(out_v, result.at[0], loc.at[12]).wait()


def on_device(mesh, *args):
    (
        latent,
        cond,
        context,
        cond_ctx,
        w_shift,
        w_scale,
        w_gate,
        norm_gain,
        w_query,
        w_key,
        w_value,
        query_gain,
        key_gain,
        ctx_lift,
        out_gain,
        w_out,
    ) = args
    n_sp, n_tp = mesh.shape["sp"], mesh.shape["tp"]
    assert n_tp == 4 and KV_HEADS == n_tp and n_sp % 4 == 0
    assert w_shift.shape == (128, 512)
    tok, width = latent.shape[1:]
    n_ctx = context.shape[1]
    rows = n_ctx + n_tp * tok
    seq = n_tp * tok
    slots = n_sp // 2 + 1
    any_ = pl.BlockSpec(memory_space=pl.ANY)
    smem = pl.BlockSpec(memory_space=pltpu.SMEM)
    dma = pltpu.SemaphoreType.DMA
    scratch = [
        pltpu.VMEM((1, width), BF16),
        pltpu.VMEM((width // 128, 128), BF16),
        pltpu.VMEM((1, width), F32),
        pltpu.VMEM((1, HEAD_DIM), F32),
        pltpu.VMEM((1, HEAD_DIM), F32),
        pltpu.VMEM((1, HEADS * HEAD_DIM), F32),
        pltpu.VMEM((n_tp, tok, width), BF16),
        pltpu.VMEM((n_ctx, width), BF16),
        pltpu.VMEM((3,) + w_shift.shape, BF16),
        pltpu.VMEM(w_query.shape, BF16),
        pltpu.VMEM((width, 2 * HEAD_DIM), BF16),
        pltpu.VMEM(w_out.shape, BF16),
        pltpu.VMEM((2, 16, 128), F32),
        pltpu.VMEM((n_sp - 1, 16, 128), F32),
        pltpu.VMEM((10, 128), F32),
        pltpu.VMEM((n_tp, 2, 16, 128), F32),
        pltpu.VMEM((8, width), F32),
        pltpu.VMEM((rows, width), F32),
        pltpu.VMEM((rows, width), BF16),
        pltpu.VMEM((rows, HEAD_DIM), F32),
        pltpu.VMEM((rows, HEAD_DIM), F32),
        pltpu.VMEM((slots, 2, rows, HEAD_DIM), BF16),
        pltpu.VMEM((slots, 2, rows, HEAD_DIM), BF16),
        pltpu.VMEM((2, seq, HEAD_DIM), BF16),
        pltpu.VMEM((2, seq, 1), F32),
        pltpu.VMEM((2, seq, 1), F32),
        pltpu.VMEM((2, seq, HEAD_DIM), F32),
        pltpu.VMEM((n_tp, tok, 2 * HEAD_DIM), BF16),
        pltpu.VMEM((n_tp, tok, 2 * HEAD_DIM), BF16),
        pltpu.VMEM((tok, HEADS * HEAD_DIM), BF16),
        pltpu.VMEM((tok, width), BF16),
        dma((13,)),
        dma((1,)),
        dma((5,)),
        dma((1,)),
        dma((1,)),
        dma((1,)),
        dma((7,)),
        dma((4,)),
        dma((2, slots - 1, 4)),
        dma((1,)),
        dma((3,)),
    ]
    specs = [any_] * 13 + [smem, any_, any_]
    row = lambda a: a.reshape(1, -1)
    return pl.pallas_call(
        functools.partial(kernel, n_sp),
        out_shape=jax.ShapeDtypeStruct(latent.shape, BF16),
        in_specs=specs,
        out_specs=any_,
        scratch_shapes=scratch,
        compiler_params=pltpu.CompilerParams(
            collective_id=0, has_side_effects=True, vmem_limit_bytes=56 << 20
        ),
    )(
        latent,
        cond,
        context,
        cond_ctx.reshape(-1, 128),
        w_shift,
        w_scale,
        w_gate,
        row(norm_gain),
        w_query,
        w_key,
        w_value,
        row(query_gain),
        row(key_gain),
        ctx_lift,
        row(out_gain),
        w_out,
    )


def solution(mesh):
    in_specs = (
        P(("grp", "dp"), ("sp", "tp"), None),
        P(("grp", "dp"), None),
        P(("grp", "dp"), "sp", None),
        P(),
        P("sp", "tp"),
        P("sp", "tp"),
        P("sp", "tp"),
        P(),
        P(None, "tp"),
        P(None, "tp"),
        P(None, "tp"),
        P(),
        P(),
        P("tp"),
        P(),
        P(),
    )
    out_specs = P(("grp", "dp"), ("sp", "tp"), None)
    return jax.shard_map(
        functools.partial(on_device, mesh),
        mesh=mesh,
        in_specs=in_specs,
        out_specs=out_specs,
        check_vma=False,
    )
```

time: 96.1 us -> 88.7 us (0.923)
  Pallas kernels: 92.8 us -> 86.7 us
  local copies, waits for them, and re-layouts: 3.06 us -> 1.77 us
    pallas_call x1, Pallas kernels: 92.8 us -> 86.7 us  [on_device(): pl.pallas_call(functools.partial(kernel, n_sp), out_shape=jax.ShapeDtypeS...]
    reshape x1 -> x0, local copies, waits for them, and re-layouts: 1.29 us -> none  [on_device(): row = lambda a: a.reshape(1, -1)]
where the time goes in v2:
time: 88.7 us; the launch traced here: 88.5 us
  Pallas kernels  86.7 us (98%)
  local copies, waits for them, and re-layouts  1.77 us (2%)
    pallas_call x1, Pallas kernels, on_device(): pl.pallas_call(functools.partial(kernel, n_sp), out_shape=jax.ShapeDtypeS...  86.7 us

profile of v2, /device:TPU:40, one launch (start us, length us, event | category | flops | bytes accessed | tf_op | source)
XLA Modules:
  0.0 88.5 jit_solution(7661438150757869786)
XLA Ops:
  0.0 86.7 %shard_map.154 = bf16[1,96,2048]{2,1,0:T(8,128)(2,1)} custom-call(bf16[1,96,2048]{2,1,0:T(8,128)(2,1)} %latent.1, bf16[1,2048]{1,0:T(2,128)(2,1)} %cond_h.1, bf16[1,16,2048]{2,1,0:T(8,128)(2,1)} %context.1, bf16[16,128]{1,0:T(8,128)(2,1)} %bitcast.6, bf16[128,512]{1,0:T(8,128)(2,1)} %w_shift.1, bf16[128,512]{1,0:T(8,128)(2,1)} %w_scale.1, ...), custom_call_target="tpu_custom_call" | custom-call | tf_op jit(solution)/shard_map/pallas_call | solution.py:569
  86.8 1.8 %copy.18 = bf16[1,96,2048]{2,1,0:T(8,128)(2,1)} copy(bf16[1,96,2048]{2,1,0:T(8,128)(2,1)} %shard_map.154) | data formatting | bytes 786432

commit v3 on v2

--- a/solution.py
+++ b/solution.py
@@ -53,6 +53,8 @@
     wo,
     part,
     got_mod,
+    window,
+    got_half,
     own_mod,
     mod_all,
     rows_mod,
@@ -69,12 +71,13 @@
     att_send,
     att_all,
     att_n,
-    out_v,
     loc,
     x_send,
     x_recv,
     p1_send,
     p1_recv,
+    h_send,
+    h_recv,
     p2_send,
     p2_recv,
     r_send,
@@ -91,6 +94,7 @@
     seq = n_tp * tok
     rows = n_ctx + seq
     width = lat.shape[2]
+    reach = n_sp // 4
     mate = z + 1 - 2 * lax.rem(z, 2)
     parity = lax.rem(z, 2)
 
@@ -125,7 +129,9 @@
     for d in range(1, n_tp):
         greet(tp=tp(d))
         greet(tp=tp(d), sp=mate)
-    each(1, n_sp, lambda d: greet(sp=lax.rem(z + d, n_sp)))
+    for d in range(1, reach + 1):
+        greet(sp=sp(d))
+        greet(sp=sp(-d))
 
     def load(src, dst, i):
         copy = pltpu.make_async_copy(src, dst, loc.at[i])
@@ -176,21 +182,22 @@
                     part[block, row : row + 1, :] = product[who : who + 1, at : at + 128]
 
     load_lat.wait()
-    pl.semaphore_wait(barrier, n_sp - 1 + 2 * (n_tp - 1))
+    pl.semaphore_wait(barrier, 2 * reach + 2 * (n_tp - 1))
 
     used = pl.ds(0, 10)
-
-    def p1(d):
-        to = lax.rem(z + d, n_sp)
-        return remote(
-            part.at[lax.rem(to, 2), used],
-            got_mod.at[d - 1, used],
+    offsets = [o for i in range(reach, 0, -1) for o in (i, -i) if o > -reach]
+    p1 = [
+        remote(
+            part.at[lax.rem(sp(-o), 2), used],
+            got_mod.at[i, used],
             p1_send.at[0],
             p1_recv.at[0],
-            sp=to,
+            sp=sp(-o),
         )
-
-    each(1, n_sp, lambda d: p1(d).start())
+        for i, o in enumerate(offsets)
+    ]
+    for copy in p1:
+        copy.start()
 
     lo, hi = pl.ds(0, half), pl.ds(half, half)
     x_copies = [
@@ -239,9 +246,16 @@
 
     every_got = got_mod.at[:, used]
     remote(every_got, every_got, p1_send.at[0], p1_recv.at[0], sp=mate).wait_recv()
-    own_mod[...] = lax.fori_loop(
-        0, n_sp - 1, lambda i, total: total + got_mod[i, 0:10, :], part[parity, 0:10, :]
-    )
+    window[...] = sum((got_mod[i, 0:10, :] for i in range(len(p1))), part[parity, 0:10, :])
+    halves = [
+        remote(window, got_half.at[i], h_send.at[0], h_recv.at[i], sp=sp(d))
+        for i, d in enumerate((reach, -reach))
+    ]
+    for copy in halves:
+        copy.start()
+    for copy in halves:
+        copy.wait_recv()
+    own_mod[...] = got_half[0] + got_half[1]
     mod_all[x, parity, 0:10, :] = own_mod[...]
     spread = [(d, e) for e in (1, 0) for d in (2, 1, 3, 0) if (d, e) != (0, 0)]
     p2 = []
@@ -413,25 +427,21 @@
         return carry
 
     lax.fori_loop(2, last, step, 0)
-    for g in range(2):
-        attend(g, pair(last - 1, 0), pair(last - 1, 1))
-
-    def chunk(way, kind, j):
-        at = n_ctx + j * tok
-        return (kv_r if way == 0 else kv_l)[last, kind, at : at + tok]
-
-    def ending(kind):
-        parts = [chunk(0, kind, 0), chunk(1, kind, 2)]
-        parts += [kv_r[s, kind, 0:n_ctx] for s in range(last + 1)]
+
+    def joined(kind):
+        parts = [kv_r[last - 1, kind, body_rows], kv_l[last - 1, kind, body_rows]]
+        parts += [kv_r[s, kind, 0:n_ctx] for s in range(last)]
         parts += [kv_l[s, kind, 0:n_ctx] for s in range(1, last)]
         return jnp.concatenate(parts, 0)
 
-    pull(last, 0)
-    pull(last, 2)
     for g in range(2):
-        attend(g, ending(0), ending(1), lift_from=2 * tok)
-    pull(last, 1)
-    pull(last, 3)
+        attend(g, joined(0), joined(1), lift_from=2 * seq)
+
+    cut = bounds[2][0]
+
+    def ending(kind):
+        parts = [kv_r[last, kind, n_ctx:cut], kv_l[last, kind, cut:rows], kv_r[last, kind, 0:n_ctx]]
+        return jnp.concatenate(parts, 0)
 
     def exchange(g, j):
         part_of = pl.ds(g * HEAD_DIM, HEAD_DIM)
@@ -443,15 +453,14 @@
             tp=tp(RELATIVE[j]),
         )
 
+    for j in range(n_tp):
+        pull(last, j)
     for g in range(2):
-        attend(
-            g,
-            jnp.concatenate([chunk(0, 0, 1), chunk(1, 0, 3)], 0),
-            jnp.concatenate([chunk(0, 1, 1), chunk(1, 1, 3)], 0),
-        )
+        attend(g, ending(0), ending(1), lift_from=seq)
         att = (acc_s[g] / l_s[g]).astype(BF16)
         for j in range(n_tp):
             att_send[j, :, g * HEAD_DIM : (g + 1) * HEAD_DIM] = att[j * tok : (j + 1) * tok]
+    for g in range(2):
         for j in (3, 1, 2):
             exchange(g, j).start()
     att_all[x] = att_send[0]
@@ -472,8 +481,7 @@
     for i in range(width // strip):
         at = pl.ds(i * strip, strip)
         mix = jnp.dot(att_n[...], wo[:, at], preferred_element_type=F32)
-        out_v[:, at] = (lat[0, :, at].astype(F32) + rows_mod[4:5, at] * mix).astype(BF16)
-        pltpu.make_async_copy(out_v.at[:, at], result.at[0, :, at], loc.at[12]).start()
+        result[0, :, at] = (lat[0, :, at].astype(F32) + rows_mod[4:5, at] * mix).astype(BF16)
 
     def sent(whole, sem):
         remote(whole, whole, sem, p1_recv.at[0], sp=mate).wait_send()
@@ -481,13 +489,13 @@
     sent(lat.at[0:3], x_send.at[0])
     sent(every_got, p1_send.at[0])
     sent(got_mod.at[0 : len(p2), used], p2_send.at[0])
+    sent(got_half, h_send.at[0])
     sent(kv_r.at[0 : last - 1], r_send.at[0])
     sent(kv_l.at[0 : last - 1], r_send.at[1])
     at, _ = bounds[2]
     sent(kv_r.at[last - 1, :, 0:at], r_send.at[2])
     sent(kv_l.at[last - 1, :, at:rows], r_send.at[3])
     sent(att_send.at[1:n_tp], o_send.at[0])
-    pltpu.make_async_copy(out_v, result.at[0], loc.at[12]).wait()
 
 
 def on_device(mesh, *args):
@@ -534,7 +542,9 @@
         pltpu.VMEM((width, 2 * HEAD_DIM), BF16),
         pltpu.VMEM(w_out.shape, BF16),
         pltpu.VMEM((2, 16, 128), F32),
-        pltpu.VMEM((n_sp - 1, 16, 128), F32),
+        pltpu.VMEM((n_sp // 2 - 1, 16, 128), F32),
+        pltpu.VMEM((10, 128), F32),
+        pltpu.VMEM((2, 10, 128), F32),
         pltpu.VMEM((10, 128), F32),
         pltpu.VMEM((n_tp, 2, 16, 128), F32),
         pltpu.VMEM((8, width), F32),
@@ -551,12 +561,13 @@
         pltpu.VMEM((n_tp, tok, 2 * HEAD_DIM), BF16),
         pltpu.VMEM((n_tp, tok, 2 * HEAD_DIM), BF16),
         pltpu.VMEM((tok, HEADS * HEAD_DIM), BF16),
-        pltpu.VMEM((tok, width), BF16),
-        dma((13,)),
+        dma((12,)),
         dma((1,)),
         dma((5,)),
         dma((1,)),
         dma((1,)),
+        dma((1,)),
+        dma((2,)),
         dma((1,)),
         dma((7,)),
         dma((4,)),
@@ -568,9 +579,9 @@
     row = lambda a: a.reshape(1, -1)
     return pl.pallas_call(
         functools.partial(kernel, n_sp),
-        out_shape=jax.ShapeDtypeStruct(latent.shape, BF16),
+        out_shape=pltpu.VMEM(latent.shape, BF16),
         in_specs=specs,
-        out_specs=any_,
+        out_specs=pl.BlockSpec(memory_space=pltpu.VMEM),
         scratch_shapes=scratch,
         compiler_params=pltpu.CompilerParams(
             collective_id=0, has_side_effects=True, vmem_limit_bytes=56 << 20

time: 88.7 us -> 84.1 us (0.948)
  Pallas kernels: 86.7 us -> 83.3 us
  local copies, waits for them, and re-layouts: 1.77 us -> 0.75 us
    pallas_call x1, Pallas kernels: 86.7 us -> 83.3 us  [on_device(): pl.pallas_call(functools.partial(kernel, n_sp), out_shape=pltpu.VMEM(late...]
    unnamed x1, local copies, waits for them, and re-layouts: 1.77 us -> 0.75 us
where the time goes in v3:
time: 84.1 us; the launch traced here: 84 us
  Pallas kernels  83.3 us (99%)
    pallas_call x1, Pallas kernels, on_device(): pl.pallas_call(functools.partial(kernel, n_sp), out_shape=pltpu.VMEM(late...  83.3 us

profile of v3, /device:TPU:40, one launch (start us, length us, event | category | flops | bytes accessed | tf_op | source)
XLA Modules:
  0.0 84.0 jit_solution(3166382854339394241)
XLA Ops:
  0.0 83.3 %shard_map.154 = bf16[1,96,2048]{2,1,0:T(8,128)(2,1)S(1)} custom-call(bf16[1,96,2048]{2,1,0:T(8,128)(2,1)} %latent.1, bf16[1,2048]{1,0:T(2,128)(2,1)} %cond_h.1, bf16[1,16,2048]{2,1,0:T(8,128)(2,1)} %context.1, bf16[16,128]{1,0:T(8,128)(2,1)} %bitcast.6, bf16[128,512]{1,0:T(8,128)(2,1)} %w_shift.1, bf16[128,512]{1,0:T(8,128)(2,1)} %w_scale.1, ...), custom_call_target="tpu_custom_call" | custom-call | tf_op jit(solution)/shard_map/pallas_call | solution.py:580
  83.3 0.7 copy.18

commit v4 on v3

--- a/solution.py
+++ b/solution.py
@@ -65,6 +65,7 @@
     kv_r,
     kv_l,
     q_s,
+    lift_s,
     m_s,
     l_s,
     acc_s,
@@ -228,6 +229,11 @@
         sine = jnp.sin(angle)
         sin_t[at : at + tok, :] = jnp.where(lower, -sine, sine)
 
+    for g in range(2):
+        lift = (ctx_lift[g] + math.log(seq / n_ctx)) * LOG2E
+        for j in range(n_tp):
+            lift_s[pl.ds((2 * j + g) * tok, tok)] = jnp.full((tok, 1), lift, F32)
+
     def prepare(read, base, count):
         def body(i, carry):
             floats = read(pl.ds(pl.multiple_of(i * 16, 16), 16)).astype(F32)
@@ -357,26 +363,35 @@
     factor = LOG2E * HEAD_DIM ** (-0.5)
     nt = (((1,), (1,)), ((), ()))
 
-    def attend(g, keys, values, first=False, lift_from=None):
-        scores = lax.dot_general(q_s[g], keys, nt, preferred_element_type=F32) * factor
-        if lift_from is not None:
-            lift = (ctx_lift[g] + math.log(seq / n_ctx)) * LOG2E
-            at = lax.broadcasted_iota(jnp.int32, (1, keys.shape[0]), 1)
-            scores = scores + jnp.where(at >= lift_from, lift, 0.0)
+    def attend(at, count, keys, values, extra=None, first=False, final=False):
+        here = pl.ds(at, count)
+        queries = q_s[here]
+        scores = lax.dot_general(queries, keys, nt, preferred_element_type=F32) * factor
+        if extra is not None:
+            more = lax.dot_general(queries, extra[0], nt, preferred_element_type=F32) * factor
+            scores = jnp.concatenate([scores, more + lift_s[here]], 1)
+            values = jnp.concatenate([values, extra[1]], 0)
         top = jnp.max(scores, -1, keepdims=True)
         if not first:
-            before = m_s[g]
+            before = m_s[here]
             top = jnp.maximum(before, top)
         weights = jnp.exp2(scores - top)
-        total = jnp.sum(weights, -1, keepdims=True)
+        full = weights.shape[1] // 128 * 128
+        total = sum(weights[:, i : i + 128] for i in range(0, full, 128))
+        if full < weights.shape[1]:
+            rest = jnp.sum(weights[:, full:], -1, keepdims=True)
+            one = lax.broadcasted_iota(jnp.int32, total.shape, 1) == 0
+            total = total + jnp.where(one, rest, 0.0)
         out = jnp.dot(weights.astype(BF16), values, preferred_element_type=F32)
         if not first:
             keep = jnp.exp2(before - top)
-            total = total + l_s[g] * keep
-            out = out + acc_s[g] * keep
-        m_s[g] = top
-        l_s[g] = total
-        acc_s[g] = out
+            total = total + l_s[here] * keep
+            out = out + acc_s[here] * keep
+        if final:
+            return (out / jnp.sum(total, -1, keepdims=True)).astype(BF16)
+        m_s[here] = top
+        l_s[here] = total
+        acc_s[here] = out
 
     def pull(s, j):
         for way in range(2):
@@ -407,76 +422,96 @@
     load_query_gain.wait()
     made = jnp.dot(normed[n_ctx:rows, :], wq[...], preferred_element_type=F32)
     for g in range(2):
-        q_s[g] = rotate(
+        turned = rotate(
             head_norm(made[:, g * HEAD_DIM : (g + 1) * HEAD_DIM], query_gain[...]), n_ctx, seq
         ).astype(BF16)
+        for j in range(n_tp):
+            q_s[pl.ds((2 * j + g) * tok, tok)] = turned[j * tok : (j + 1) * tok]
     pull(1, 1)
-    attend(0, kv_r[0, 0, body_rows], kv_r[0, 1, body_rows], first=True)
+    for part_of in range(2):
+        attend(part_of * seq, seq, kv_r[0, 0, body_rows], kv_r[0, 1, body_rows], first=True)
     pull(1, 2)
     pull(1, 3)
-    attend(1, kv_r[0, 0, body_rows], kv_r[0, 1, body_rows], first=True)
-
-    def pair(slot, kind):
+
+    def both(slot, kind):
         return jnp.concatenate([kv_r[slot, kind, body_rows], kv_l[slot, kind, body_rows]], 0)
 
     def step(s, carry):
-        for g in range(2):
-            for j in (2 * g, 2 * g + 1):
-                pull(s, j)
-            attend(g, pair(s - 1, 0), pair(s - 1, 1))
+        for part_of in range(2):
+            pull(s, 2 * part_of)
+            pull(s, 2 * part_of + 1)
+            attend(part_of * seq, seq, both(s - 1, 0), both(s - 1, 1))
         return carry
 
     lax.fori_loop(2, last, step, 0)
 
-    def joined(kind):
-        parts = [kv_r[last - 1, kind, body_rows], kv_l[last - 1, kind, body_rows]]
-        parts += [kv_r[s, kind, 0:n_ctx] for s in range(last)]
+    def contexts(kind):
+        parts = [kv_r[s, kind, 0:n_ctx] for s in range(last)]
         parts += [kv_l[s, kind, 0:n_ctx] for s in range(1, last)]
         return jnp.concatenate(parts, 0)
 
-    for g in range(2):
-        attend(g, joined(0), joined(1), lift_from=2 * seq)
+    for part_of in range(2):
+        attend(
+            part_of * seq,
+            seq,
+            both(last - 1, 0),
+            both(last - 1, 1),
+            extra=(contexts(0), contexts(1)),
+        )
 
     cut = bounds[2][0]
 
     def ending(kind):
-        parts = [kv_r[last, kind, n_ctx:cut], kv_l[last, kind, cut:rows], kv_r[last, kind, 0:n_ctx]]
-        return jnp.concatenate(parts, 0)
-
-    def exchange(g, j):
-        part_of = pl.ds(g * HEAD_DIM, HEAD_DIM)
-        return remote(
-            att_send.at[j, :, part_of],
-            att_all.at[x, :, part_of],
-            o_send.at[0],
-            o_recv.at[j - 1],
-            tp=tp(RELATIVE[j]),
-        )
+        return jnp.concatenate([kv_r[last, kind, n_ctx:cut], kv_l[last, kind, cut:rows]], 0)
 
     for j in range(n_tp):
         pull(last, j)
-    for g in range(2):
-        attend(g, ending(0), ending(1), lift_from=seq)
-        att = (acc_s[g] / l_s[g]).astype(BF16)
-        for j in range(n_tp):
-            att_send[j, :, g * HEAD_DIM : (g + 1) * HEAD_DIM] = att[j * tok : (j + 1) * tok]
-    for g in range(2):
-        for j in (3, 1, 2):
-            exchange(g, j).start()
-    att_all[x] = att_send[0]
+    sends = []
+    for j in (3, 1, 2, 0):
+        att = attend(
+            2 * j * tok,
+            2 * tok,
+            ending(0),
+            ending(1),
+            extra=(kv_r[last, 0, 0:n_ctx], kv_r[last, 1, 0:n_ctx]),
+            final=True,
+        )
+        for g in range(2):
+            half_att = att[g * tok : (g + 1) * tok]
+            if j == 0:
+                att_all[x, :, pl.ds(g * HEAD_DIM, HEAD_DIM)] = half_att
+            else:
+                att_send[j - 1, :, pl.ds(g * HEAD_DIM, HEAD_DIM)] = half_att
+        if j > 0:
+            copy = remote(
+                att_send.at[j - 1],
+                att_all.at[x],
+                o_send.at[0],
+                o_recv.at[j - 1],
+                tp=tp(RELATIVE[j]),
+            )
+            copy.start()
     load_wo.wait()
     load_out_gain.wait()
-    for j in range(1, n_tp):
-        whole = att_all.at[tp(-RELATIVE[j])]
+
+    def channel_block(b):
+        floats = att_all[b].astype(F32)
+        return jnp.sum(floats * floats, -1, keepdims=True)
+
+    square = channel_block(x)
+    for j in (1, 2, 3):
+        source = tp(-RELATIVE[j])
+        whole = att_all.at[source]
         remote(whole, whole, o_send.at[0], o_recv.at[j - 1], tp=tp(1)).wait_recv()
+        square = square + channel_block(source)
 
     channels = att_all.shape[2]
-    pieces = [att_all[b].astype(F32) for b in range(n_tp)]
-    square = sum(jnp.sum(p * p, -1, keepdims=True) for p in pieces)
     inv = lax.rsqrt(square * (1.0 / (n_tp * channels)) + EPSILON)
     for b in range(n_tp):
         gain = out_gain[:, b * channels : (b + 1) * channels]
-        att_n[:, b * channels : (b + 1) * channels] = (pieces[b] * inv * gain).astype(BF16)
+        att_n[:, b * channels : (b + 1) * channels] = (
+            att_all[b].astype(F32) * inv * gain
+        ).astype(BF16)
     strip = 512
     for i in range(width // strip):
         at = pl.ds(i * strip, strip)
@@ -495,7 +530,7 @@
     at, _ = bounds[2]
     sent(kv_r.at[last - 1, :, 0:at], r_send.at[2])
     sent(kv_l.at[last - 1, :, at:rows], r_send.at[3])
-    sent(att_send.at[1:n_tp], o_send.at[0])
+    sent(att_send, o_send.at[0])
 
 
 def on_device(mesh, *args):
@@ -554,11 +589,12 @@
         pltpu.VMEM((rows, HEAD_DIM), F32),
         pltpu.VMEM((slots, 2, rows, HEAD_DIM), BF16),
         pltpu.VMEM((slots, 2, rows, HEAD_DIM), BF16),
-        pltpu.VMEM((2, seq, HEAD_DIM), BF16),
-        pltpu.VMEM((2, seq, 1), F32),
-        pltpu.VMEM((2, seq, 1), F32),
-        pltpu.VMEM((2, seq, HEAD_DIM), F32),
-        pltpu.VMEM((n_tp, tok, 2 * HEAD_DIM), BF16),
+        pltpu.VMEM((2 * seq, HEAD_DIM), BF16),
+        pltpu.VMEM((2 * seq, 1), F32),
+        pltpu.VMEM((2 * seq, 1), F32),
+        pltpu.VMEM((2 * seq, 128), F32),
+        pltpu.VMEM((2 * seq, HEAD_DIM), F32),
+        pltpu.VMEM((n_tp - 1, tok, 2 * HEAD_DIM), BF16),
         pltpu.VMEM((n_tp, tok, 2 * HEAD_DIM), BF16),
         pltpu.VMEM((tok, HEADS * HEAD_DIM), BF16),
         dma((12,)),

time: 84.1 us -> 83.5 us (level)
  no operation moved by 1% of the time
where the time goes in v4:
time: 83.5 us; the launch traced here: 83.4 us
  Pallas kernels  82.6 us (99%)
    pallas_call x1, Pallas kernels, on_device(): pl.pallas_call(functools.partial(kernel, n_sp), out_shape=pltpu.VMEM(late...  82.6 us

profile of v4, /device:TPU:40, one launch (start us, length us, event | category | flops | bytes accessed | tf_op | source)
XLA Modules:
  0.0 83.4 jit_solution(6079860455195812905)
XLA Ops:
  0.0 82.6 %shard_map.154 = bf16[1,96,2048]{2,1,0:T(8,128)(2,1)S(1)} custom-call(bf16[1,96,2048]{2,1,0:T(8,128)(2,1)} %latent.1, bf16[1,2048]{1,0:T(2,128)(2,1)} %cond_h.1, bf16[1,16,2048]{2,1,0:T(8,128)(2,1)} %context.1, bf16[16,128]{1,0:T(8,128)(2,1)} %bitcast.6, bf16[128,512]{1,0:T(8,128)(2,1)} %w_shift.1, bf16[128,512]{1,0:T(8,128)(2,1)} %w_scale.1, ...), custom_call_target="tpu_custom_call" | custom-call | tf_op jit(solution)/shard_map/pallas_call | solution.py:616
  82.6 0.7 copy.18

commit v5 on v4

--- a/solution.py
+++ b/solution.py
@@ -52,7 +52,7 @@
     wkv,
     wo,
     part,
-    got_mod,
+    both_got,
     window,
     got_half,
     own_mod,
@@ -88,6 +88,7 @@
 ):
     z = lax.axis_index("sp")
     x = lax.axis_index("tp")
+    core = lax.axis_index("dp")
     n_tp = 4
     tok = lat.shape[1]
     half = tok // 2
@@ -96,6 +97,8 @@
     rows = n_ctx + seq
     width = lat.shape[2]
     reach = n_sp // 4
+    got_mod = both_got.at[0 : n_sp // 2 - 1]
+    got_other = both_got.at[n_sp // 2 - 1 : n_sp - 1]
     mate = z + 1 - 2 * lax.rem(z, 2)
     parity = lax.rem(z, 2)
 
@@ -127,12 +130,33 @@
     def greet(**where):
         pl.semaphore_signal(barrier, inc=1, device_id=where, device_id_type=MESH)
 
-    for d in range(1, n_tp):
-        greet(tp=tp(d))
-        greet(tp=tp(d), sp=mate)
-    for d in range(1, reach + 1):
-        greet(sp=sp(d))
-        greet(sp=sp(-d))
+    for d in range(reach, 0, -1):
+        greet(sp=sp(d), dp=1)
+        greet(sp=sp(-d), dp=1)
+    for d in (2, 1, 3):
+        greet(tp=tp(d), sp=mate, dp=1)
+        greet(tp=tp(d), dp=1)
+
+    @pl.when(core == 0)
+    def _():
+        greet(sp=sp(1))
+        greet(sp=sp(-1))
+        for d in range(1, n_tp):
+            greet(tp=tp(d))
+        greet(dp=1)
+
+    @pl.when(core == 1)
+    def _():
+        for d in range(reach, 0, -1):
+            greet(sp=sp(d), dp=0)
+            greet(sp=sp(-d), dp=0)
+        for d in (2, 1, 3):
+            greet(tp=tp(d), sp=mate, dp=0)
+            greet(tp=tp(d), dp=0)
+        greet(dp=0)
+
+    common = 2 * reach + 2 * (n_tp - 1)
+    greeted = jnp.where(core == 0, common + 2 + n_tp, 2 * common + 1)
 
     def load(src, dst, i):
         copy = pltpu.make_async_copy(src, dst, loc.at[i])
@@ -183,22 +207,30 @@
                     part[block, row : row + 1, :] = product[who : who + 1, at : at + 128]
 
     load_lat.wait()
-    pl.semaphore_wait(barrier, 2 * reach + 2 * (n_tp - 1))
+    pl.semaphore_wait(barrier, greeted)
 
     used = pl.ds(0, 10)
     offsets = [o for i in range(reach, 0, -1) for o in (i, -i) if o > -reach]
-    p1 = [
-        remote(
+
+    def p1(own, i, o):
+        return remote(
             part.at[lax.rem(sp(-o), 2), used],
-            got_mod.at[i, used],
+            (got_mod if own else got_other).at[i, used],
             p1_send.at[0],
-            p1_recv.at[0],
+            p1_recv.at[0 if own else 1],
             sp=sp(-o),
+            dp=1,
         )
-        for i, o in enumerate(offsets)
-    ]
-    for copy in p1:
-        copy.start()
+
+    @pl.when(core == 1)
+    def _():
+        for i, o in enumerate(offsets):
+            p1(True, i, o).start()
+
+    @pl.when(core == 0)
+    def _():
+        for i, o in enumerate(offsets + [0]):
+            p1(False, i, o).start()
 
     lo, hi = pl.ds(0, half), pl.ds(half, half)
     x_copies = [
@@ -250,43 +282,70 @@
     load_gain.wait()
     load_key_gain.wait()
 
-    every_got = got_mod.at[:, used]
-    remote(every_got, every_got, p1_send.at[0], p1_recv.at[0], sp=mate).wait_recv()
-    window[...] = sum((got_mod[i, 0:10, :] for i in range(len(p1))), part[parity, 0:10, :])
-    halves = [
-        remote(window, got_half.at[i], h_send.at[0], h_recv.at[i], sp=sp(d))
-        for i, d in enumerate((reach, -reach))
-    ]
-    for copy in halves:
-        copy.start()
-    for copy in halves:
-        copy.wait_recv()
-    own_mod[...] = got_half[0] + got_half[1]
-    mod_all[x, parity, 0:10, :] = own_mod[...]
-    spread = [(d, e) for e in (1, 0) for d in (2, 1, 3, 0) if (d, e) != (0, 0)]
-    p2 = []
-    for i, (d, e) in enumerate(spread):
-        where = {}
+    own_got = got_mod.at[:, used]
+    other_got = got_other.at[:, used]
+
+    def half_window(own, i):
+        return remote(
+            window.at[0 if own else 1],
+            got_half.at[i if own else 2 + i],
+            h_send.at[0],
+            h_recv.at[i if own else 2 + i],
+            sp=sp((reach, -reach)[i]),
+        )
+
+    spread = [(d, e) for e in (1, 0) for d in (2, 1, 3, 0)]
+
+    def p2(core_of, i):
+        d, e = spread[i]
+        where = dict(dp=core_of)
         if d:
             where["tp"] = tp(d)
         if e:
             where["sp"] = mate
-        p2.append(
-            remote(own_mod, mod_all.at[x, parity, used], p2_send.at[0], p2_recv.at[i], **where)
+        return remote(
+            own_mod.at[1 - core_of],
+            mod_all.at[x, parity, used],
+            p2_send.at[0],
+            p2_recv.at[i],
+            **where,
         )
-    for copy in p2:
-        copy.start()
+
+    @pl.when(core == 1)
+    def _():
+        remote(own_got, own_got, p1_send.at[0], p1_recv.at[0], sp=mate).wait_recv()
+        window[0] = sum((got_mod[i, 0:10, :] for i in range(len(offsets))), part[parity, 0:10, :])
+        for i in range(2):
+            half_window(True, i).start()
+        remote(other_got, other_got, p1_send.at[0], p1_recv.at[1], sp=mate).wait_recv()
+        window[1] = sum(got_other[i, 0:10, :] for i in range(len(offsets) + 1))
+        for i in range(2):
+            half_window(False, i).start()
+        for i in range(2):
+            half_window(True, i).wait_recv()
+        own_mod[0] = got_half[0] + got_half[1]
+        mod_all[x, parity, 0:10, :] = own_mod[0]
+        for i in range(7):
+            p2(1, i).start()
+        for i in range(2):
+            half_window(False, i).wait_recv()
+        own_mod[1] = got_half[2] + got_half[3]
+        for i in range(8):
+            p2(0, i).start()
 
     x_copies[0].wait_recv()
     x_copies[4].start()
     x_copies[1].wait_recv()
     x_copies[5].start()
-    x_copies[2].wait_recv()
-    prepare(lambda i: lat[1, i, :], n_ctx + tok, tok)
-    x_copies[3].wait_recv()
-    prepare(lambda i: lat[2, i, :], n_ctx + 2 * tok, tok)
-    for copy in p2:
-        copy.wait_recv()
+    prepare(lambda i: lat[1, i, :], n_ctx + tok, half)
+    prepare(lambda i: lat[2, pl.ds(half + i.start, i.size), :], n_ctx + 2 * tok + half, half)
+    for i in range(7):
+        p2(1, i).wait_recv()
+
+    @pl.when(core == 0)
+    def _():
+        p2(0, 7).wait_recv()
+
 
     cols = width // n_tp
     for b in range(n_tp):
@@ -318,14 +377,24 @@
         floats = raw.astype(BF16).astype(F32)
         return floats * lax.rsqrt(jnp.mean(floats * floats, -1, keepdims=True) + EPSILON) * gain
 
-    def rotate(vectors, at, count):
-        d = lax.broadcasted_iota(jnp.int32, (count, HEAD_DIM), 1)
+    def rotate(vectors, pieces):
+        d = lax.broadcasted_iota(jnp.int32, vectors.shape, 1)
+        cosine = jnp.concatenate([cos_t[b : b + n, :] for b, n in pieces], 0)
+        sine = jnp.concatenate([sin_t[b : b + n, :] for b, n in pieces], 0)
         swapped = jnp.where(
             (d & (2 * quarter - 1)) < quarter,
             pltpu.roll(vectors, HEAD_DIM - quarter, 1),
             pltpu.roll(vectors, quarter, 1),
         )
-        return vectors * cos_t[at : at + count, :] + swapped * sin_t[at : at + count, :]
+        return vectors * cosine + swapped * sine
+
+    second, third = n_ctx + tok, n_ctx + 2 * tok
+    chunk_rows = [
+        [(0, n_ctx + tok)],
+        [(second, half), (third + half, half)],
+        [(second + half, half), (third, half)],
+        [(n_ctx + 3 * tok, tok)],
+    ]
 
     bounds = [(0, n_ctx + tok)] + [(n_ctx + j * tok, tok) for j in range(1, n_tp)]
 
@@ -342,23 +411,6 @@
             sp=target,
         )
 
-    norm_rows(0, n_ctx, 1)
-    for j in range(n_tp):
-        at, count = bounds[j]
-        if j == 3:
-            remote(lat.at[3], lat.at[3], x_send.at[0], x_recv.at[4], tp=tp(1)).wait_recv()
-            prepare(lambda i: lat[3, i, :], n_ctx + 3 * tok, tok)
-        norm_rows(n_ctx + j * tok, tok, 0)
-        made = jnp.dot(normed[at : at + count, :], wkv[...], preferred_element_type=F32)
-        keys = rotate(head_norm(made[:, :HEAD_DIM], key_gain[...]), at, count).astype(BF16)
-        values = made[:, HEAD_DIM:].astype(BF16)
-        kv_r[0, 0, at : at + count, :] = keys
-        kv_l[0, 0, at : at + count, :] = keys
-        kv_r[0, 1, at : at + count, :] = values
-        kv_l[0, 1, at : at + count, :] = values
-        ring(0, 1, j).start()
-        ring(1, 1, j).start()
-
     last = n_sp // 2
     factor = LOG2E * HEAD_DIM ** (-0.5)
     nt = (((1,), (1,)), ((), ()))
@@ -371,11 +423,13 @@
             more = lax.dot_general(queries, extra[0], nt, preferred_element_type=F32) * factor
             scores = jnp.concatenate([scores, more + lift_s[here]], 1)
             values = jnp.concatenate([values, extra[1]], 0)
-        top = jnp.max(scores, -1, keepdims=True)
+        top = jnp.broadcast_to(jnp.max(scores, -1, keepdims=True), (count, 128))
         if not first:
             before = m_s[here]
             top = jnp.maximum(before, top)
-        weights = jnp.exp2(scores - top)
+        size = scores.shape[1]
+        wide = jnp.concatenate([top] * (size // 128) + [top[:, : size % 128]] * (size % 128 > 0), 1)
+        weights = jnp.exp2(scores - wide)
         full = weights.shape[1] // 128 * 128
         total = sum(weights[:, i : i + 128] for i in range(0, full, 128))
         if full < weights.shape[1]:
@@ -416,34 +470,71 @@
             if short:
                 pl.when(s + 1 == last)(functools.partial(forward, True))
 
+    norm_rows(0, n_ctx, 1)
+    norm_rows(n_ctx, tok, 0)
+
+    def produce(j):
+        at, count = bounds[j]
+        if j == 2:
+            x_copies[2].wait_recv()
+            x_copies[3].wait_recv()
+            prepare(lambda i: lat[1, pl.ds(half + i.start, i.size), :], second + half, half)
+            prepare(lambda i: lat[2, i, :], third, half)
+        if j == 3:
+            remote(lat.at[3], lat.at[3], x_send.at[0], x_recv.at[4], tp=tp(1)).wait_recv()
+            prepare(lambda i: lat[3, i, :], n_ctx + 3 * tok, tok)
+        pieces = chunk_rows[j]
+        if j > 0:
+            for begin, size in pieces:
+                norm_rows(begin, size, 0)
+        inputs = jnp.concatenate([normed[b : b + n, :] for b, n in pieces], 0)
+        made = jnp.dot(inputs, wkv[...], preferred_element_type=F32)
+        keys = rotate(head_norm(made[:, :HEAD_DIM], key_gain[...]), pieces).astype(BF16)
+        values = made[:, HEAD_DIM:].astype(BF16)
+        kv_r[0, 0, at : at + count, :] = keys
+        kv_l[0, 0, at : at + count, :] = keys
+        kv_r[0, 1, at : at + count, :] = values
+        kv_l[0, 1, at : at + count, :] = values
+        ring(0, 1, j).start()
+        ring(1, 1, j).start()
+
     body_rows = pl.ds(n_ctx, seq)
+    produce(0)
+    produce(1)
+    produce(2)
     pull(1, 0)
+    produce(3)
+    pull(1, 1)
     load_wq.wait()
     load_query_gain.wait()
     made = jnp.dot(normed[n_ctx:rows, :], wq[...], preferred_element_type=F32)
     for g in range(2):
         turned = rotate(
-            head_norm(made[:, g * HEAD_DIM : (g + 1) * HEAD_DIM], query_gain[...]), n_ctx, seq
+            head_norm(made[:, g * HEAD_DIM : (g + 1) * HEAD_DIM], query_gain[...]), [(n_ctx, seq)]
         ).astype(BF16)
         for j in range(n_tp):
             q_s[pl.ds((2 * j + g) * tok, tok)] = turned[j * tok : (j + 1) * tok]
-    pull(1, 1)
+    pull(1, 2)
     for part_of in range(2):
         attend(part_of * seq, seq, kv_r[0, 0, body_rows], kv_r[0, 1, body_rows], first=True)
-    pull(1, 2)
-    pull(1, 3)
 
     def both(slot, kind):
         return jnp.concatenate([kv_r[slot, kind, body_rows], kv_l[slot, kind, body_rows]], 0)
 
     def step(s, carry):
         for part_of in range(2):
-            pull(s, 2 * part_of)
-            pull(s, 2 * part_of + 1)
+            if part_of == 0:
+                pull(s, 0)
+                pull(s - 1, 3)
+            else:
+                pull(s, 1)
+                pull(s, 2)
             attend(part_of * seq, seq, both(s - 1, 0), both(s - 1, 1))
         return carry
 
     lax.fori_loop(2, last, step, 0)
+    pull(last, 0)
+    pull(last - 1, 3)
 
     def contexts(kind):
         parts = [kv_r[s, kind, 0:n_ctx] for s in range(last)]
@@ -464,7 +555,7 @@
     def ending(kind):
         return jnp.concatenate([kv_r[last, kind, n_ctx:cut], kv_l[last, kind, cut:rows]], 0)
 
-    for j in range(n_tp):
+    for j in range(1, n_tp):
         pull(last, j)
     sends = []
     for j in (3, 1, 2, 0):
@@ -522,9 +613,17 @@
         remote(whole, whole, sem, p1_recv.at[0], sp=mate).wait_send()
 
     sent(lat.at[0:3], x_send.at[0])
-    sent(every_got, p1_send.at[0])
-    sent(got_mod.at[0 : len(p2), used], p2_send.at[0])
-    sent(got_half, h_send.at[0])
+
+    @pl.when(core == 0)
+    def _():
+        sent(other_got, p1_send.at[0])
+
+    @pl.when(core == 1)
+    def _():
+        sent(own_got, p1_send.at[0])
+        sent(got_half, h_send.at[0])
+        sent(both_got.at[:, used], p2_send.at[0])
+
     sent(kv_r.at[0 : last - 1], r_send.at[0])
     sent(kv_l.at[0 : last - 1], r_send.at[1])
     at, _ = bounds[2]
@@ -553,7 +652,8 @@
         w_out,
     ) = args
     n_sp, n_tp = mesh.shape["sp"], mesh.shape["tp"]
-    assert n_tp == 4 and KV_HEADS == n_tp and n_sp % 4 == 0
+    assert mesh.shape["dp"] == 2
+    assert n_tp == 4 and KV_HEADS == n_tp and n_sp == 16
     assert w_shift.shape == (128, 512)
     tok, width = latent.shape[1:]
     n_ctx = context.shape[1]
@@ -577,10 +677,10 @@
         pltpu.VMEM((width, 2 * HEAD_DIM), BF16),
         pltpu.VMEM(w_out.shape, BF16),
         pltpu.VMEM((2, 16, 128), F32),
-        pltpu.VMEM((n_sp // 2 - 1, 16, 128), F32),
-        pltpu.VMEM((10, 128), F32),
+        pltpu.VMEM((n_sp - 1, 16, 128), F32),
         pltpu.VMEM((2, 10, 128), F32),
-        pltpu.VMEM((10, 128), F32),
+        pltpu.VMEM((4, 10, 128), F32),
+        pltpu.VMEM((2, 10, 128), F32),
         pltpu.VMEM((n_tp, 2, 16, 128), F32),
         pltpu.VMEM((8, width), F32),
         pltpu.VMEM((rows, width), F32),
@@ -591,7 +691,7 @@
         pltpu.VMEM((slots, 2, rows, HEAD_DIM), BF16),
         pltpu.VMEM((2 * seq, HEAD_DIM), BF16),
         pltpu.VMEM((2 * seq, 1), F32),
-        pltpu.VMEM((2 * seq, 1), F32),
+        pltpu.VMEM((2 * seq, 128), F32),
         pltpu.VMEM((2 * seq, 128), F32),
         pltpu.VMEM((2 * seq, HEAD_DIM), F32),
         pltpu.VMEM((n_tp - 1, tok, 2 * HEAD_DIM), BF16),
@@ -601,11 +701,11 @@
         dma((1,)),
         dma((5,)),
         dma((1,)),
-        dma((1,)),
-        dma((1,)),
         dma((2,)),
         dma((1,)),
-        dma((7,)),
+        dma((4,)),
+        dma((1,)),
+        dma((8,)),
         dma((4,)),
         dma((2, slots - 1, 4)),
         dma((1,)),

time: 83.5 us -> 82.9 us (level)
  no operation moved by 1% of the time
where the time goes in v5:
time: 82.9 us; the launch traced here: 82.7 us
  Pallas kernels  82 us (99%)
    pallas_call x1, Pallas kernels, on_device(): pl.pallas_call(functools.partial(kernel, n_sp), out_shape=pltpu.VMEM(late...  82 us

profile of v5, /device:TPU:40, one launch (start us, length us, event | category | flops | bytes accessed | tf_op | source)
XLA Modules:
  0.0 82.7 jit_solution(229370152918140895)
XLA Ops:
  0.0 82.0 %shard_map.154 = bf16[1,96,2048]{2,1,0:T(8,128)(2,1)S(1)} custom-call(bf16[1,96,2048]{2,1,0:T(8,128)(2,1)} %latent.1, bf16[1,2048]{1,0:T(2,128)(2,1)} %cond_h.1, bf16[1,16,2048]{2,1,0:T(8,128)(2,1)} %context.1, bf16[16,128]{1,0:T(8,128)(2,1)} %bitcast.6, bf16[128,512]{1,0:T(8,128)(2,1)} %w_shift.1, bf16[128,512]{1,0:T(8,128)(2,1)} %w_scale.1, ...), custom_call_target="tpu_custom_call" | custom-call | tf_op jit(solution)/shard_map/pallas_call | solution.py:716
  82.0 0.7 copy.18

commit v6 on v5

--- a/solution.py
+++ b/solution.py
@@ -130,30 +130,30 @@
     def greet(**where):
         pl.semaphore_signal(barrier, inc=1, device_id=where, device_id_type=MESH)
 
-    for d in range(reach, 0, -1):
-        greet(sp=sp(d), dp=1)
-        greet(sp=sp(-d), dp=1)
-    for d in (2, 1, 3):
-        greet(tp=tp(d), sp=mate, dp=1)
-        greet(tp=tp(d), dp=1)
-
     @pl.when(core == 0)
     def _():
+        for d in range(reach, 0, -1):
+            greet(sp=sp(d), dp=1)
+            greet(sp=sp(-d), dp=1)
+        greet(dp=1)
+        for d in (2, 1, 3):
+            greet(tp=tp(d))
+            greet(tp=tp(d), dp=1)
+            greet(tp=tp(d), sp=mate, dp=1)
         greet(sp=sp(1))
         greet(sp=sp(-1))
-        for d in range(1, n_tp):
-            greet(tp=tp(d))
-        greet(dp=1)
 
     @pl.when(core == 1)
     def _():
         for d in range(reach, 0, -1):
-            greet(sp=sp(d), dp=0)
-            greet(sp=sp(-d), dp=0)
+            for to in range(2):
+                greet(sp=sp(d), dp=to)
+                greet(sp=sp(-d), dp=to)
+        greet(dp=0)
         for d in (2, 1, 3):
-            greet(tp=tp(d), sp=mate, dp=0)
-            greet(tp=tp(d), dp=0)
-        greet(dp=0)
+            for to in (1, 0):
+                greet(tp=tp(d), dp=to)
+                greet(tp=tp(d), sp=mate, dp=to)
 
     common = 2 * reach + 2 * (n_tp - 1)
     greeted = jnp.where(core == 0, common + 2 + n_tp, 2 * common + 1)
@@ -557,31 +557,32 @@
 
     for j in range(1, n_tp):
         pull(last, j)
-    sends = []
-    for j in (3, 1, 2, 0):
-        att = attend(
-            2 * j * tok,
-            2 * tok,
-            ending(0),
-            ending(1),
-            extra=(kv_r[last, 0, 0:n_ctx], kv_r[last, 1, 0:n_ctx]),
-            final=True,
-        )
-        for g in range(2):
-            half_att = att[g * tok : (g + 1) * tok]
-            if j == 0:
-                att_all[x, :, pl.ds(g * HEAD_DIM, HEAD_DIM)] = half_att
-            else:
-                att_send[j - 1, :, pl.ds(g * HEAD_DIM, HEAD_DIM)] = half_att
-        if j > 0:
-            copy = remote(
-                att_send.at[j - 1],
-                att_all.at[x],
-                o_send.at[0],
-                o_recv.at[j - 1],
-                tp=tp(RELATIVE[j]),
+    for group in ((3,), (1, 2), (0,)):
+        for j in group:
+            att = attend(
+                2 * j * tok,
+                2 * tok,
+                ending(0),
+                ending(1),
+                extra=(kv_r[last, 0, 0:n_ctx], kv_r[last, 1, 0:n_ctx]),
+                final=True,
             )
-            copy.start()
+            for g in range(2):
+                one = att[g * tok : (g + 1) * tok]
+                if j == 0:
+                    att_all[x, :, pl.ds(g * HEAD_DIM, HEAD_DIM)] = one
+                else:
+                    att_send[j - 1, :, pl.ds(g * HEAD_DIM, HEAD_DIM)] = one
+        for j in group:
+            if j > 0:
+                copy = remote(
+                    att_send.at[j - 1],
+                    att_all.at[x],
+                    o_send.at[0],
+                    o_recv.at[j - 1],
+                    tp=tp(RELATIVE[j]),
+                )
+                copy.start()
     load_wo.wait()
     load_out_gain.wait()
 

time: 82.9 us -> 82.9 us (level)
  no operation moved by 1% of the time
where the time goes in v6:
time: 82.9 us; the launch traced here: 82.8 us
  Pallas kernels  82.1 us (99%)
    pallas_call x1, Pallas kernels, on_device(): pl.pallas_call(functools.partial(kernel, n_sp), out_shape=pltpu.VMEM(late...  82.1 us

profile of v6, /device:TPU:40, one launch (start us, length us, event | category | flops | bytes accessed | tf_op | source)
XLA Modules:
  0.0 82.8 jit_solution(11314485396570119361)
XLA Ops:
  0.0 82.1 %shard_map.154 = bf16[1,96,2048]{2,1,0:T(8,128)(2,1)S(1)} custom-call(bf16[1,96,2048]{2,1,0:T(8,128)(2,1)} %latent.1, bf16[1,2048]{1,0:T(2,128)(2,1)} %cond_h.1, bf16[1,16,2048]{2,1,0:T(8,128)(2,1)} %context.1, bf16[16,128]{1,0:T(8,128)(2,1)} %bitcast.6, bf16[128,512]{1,0:T(8,128)(2,1)} %w_shift.1, bf16[128,512]{1,0:T(8,128)(2,1)} %w_scale.1, ...), custom_call_target="tpu_custom_call" | custom-call | tf_op jit(solution)/shard_map/pallas_call | solution.py:717
  82.1 0.7 copy.18

commit v7 on v6

--- a/solution.py
+++ b/solution.py
@@ -307,7 +307,7 @@
             own_mod.at[1 - core_of],
             mod_all.at[x, parity, used],
             p2_send.at[0],
-            p2_recv.at[i],
+            p2_recv.at[0],
             **where,
         )
 
@@ -339,12 +339,12 @@
     x_copies[5].start()
     prepare(lambda i: lat[1, i, :], n_ctx + tok, half)
     prepare(lambda i: lat[2, pl.ds(half + i.start, i.size), :], n_ctx + 2 * tok + half, half)
-    for i in range(7):
-        p2(1, i).wait_recv()
-
-    @pl.when(core == 0)
-    def _():
-        p2(0, 7).wait_recv()
+    for count in (7, 8):
+
+        @pl.when(core == 8 - count)
+        def _(count=count):
+            tiles = both_got.at[0:count, used]
+            remote(tiles, tiles, p2_send.at[0], p2_recv.at[0], sp=mate).wait_recv()
 
 
     cols = width // n_tp
@@ -407,7 +407,7 @@
             buf.at[slot - 1, :, piece],
             buf.at[slot, :, piece],
             r_send.at[way + 2 if final else way],
-            r_recv.at[way, slot - 1, j],
+            r_recv.at[slot - 1, j],
             sp=target,
         )
 
@@ -448,27 +448,27 @@
         acc_s[here] = out
 
     def pull(s, j):
-        for way in range(2):
-            short = (j < 2) if way == 0 else (j >= 2)
-
-            def wait(way=way):
-                ring(way, s, j).wait_recv()
-
-            def forward(final, way=way):
-                ring(way, s + 1, j, final).start()
-
-            if isinstance(s, int):
-                if s < last or short:
-                    wait()
-                if s + 1 < last:
-                    forward(False)
-                elif s + 1 == last and short:
-                    forward(True)
-                continue
-            wait()
-            pl.when(s + 1 < last)(functools.partial(forward, False))
-            if short:
-                pl.when(s + 1 == last)(functools.partial(forward, True))
+        at, count = bounds[j]
+        own_way = 0 if j < 2 else 1
+
+        def final():
+            ring(own_way, last, j, True).start()
+
+        if isinstance(s, int) and s == last:
+            ring(own_way, s, j).wait_recv()
+            return
+        pair = kv_r.at[0:2, :, pl.ds(at, count)]
+        remote(pair, pair, r_send.at[0], r_recv.at[s - 1, j], sp=mate).wait_recv()
+
+        def forward():
+            for way in range(2):
+                ring(way, s + 1, j).start()
+
+        if isinstance(s, int):
+            (forward if s + 1 < last else final)()
+        else:
+            pl.when(s + 1 < last)(forward)
+            pl.when(s + 1 == last)(final)
 
     norm_rows(0, n_ctx, 1)
     norm_rows(n_ctx, tok, 0)
@@ -706,9 +706,9 @@
         dma((1,)),
         dma((4,)),
         dma((1,)),
-        dma((8,)),
+        dma((1,)),
         dma((4,)),
-        dma((2, slots - 1, 4)),
+        dma((slots - 1, 4)),
         dma((1,)),
         dma((3,)),
     ]

time: 82.9 us -> 82.7 us (level)
  no operation moved by 1% of the time
where the time goes in v7:
time: 82.7 us; the launch traced here: 82.5 us
  Pallas kernels  81.8 us (99%)
    pallas_call x1, Pallas kernels, on_device(): pl.pallas_call(functools.partial(kernel, n_sp), out_shape=pltpu.VMEM(late...  81.8 us

profile of v7, /device:TPU:40, one launch (start us, length us, event | category | flops | bytes accessed | tf_op | source)
XLA Modules:
  0.0 82.5 jit_solution(9966512829297493967)
XLA Ops:
  0.0 81.8 %shard_map.154 = bf16[1,96,2048]{2,1,0:T(8,128)(2,1)S(1)} custom-call(bf16[1,96,2048]{2,1,0:T(8,128)(2,1)} %latent.1, bf16[1,2048]{1,0:T(2,128)(2,1)} %cond_h.1, bf16[1,16,2048]{2,1,0:T(8,128)(2,1)} %context.1, bf16[16,128]{1,0:T(8,128)(2,1)} %bitcast.6, bf16[128,512]{1,0:T(8,128)(2,1)} %w_shift.1, bf16[128,512]{1,0:T(8,128)(2,1)} %w_scale.1, ...), custom_call_target="tpu_custom_call" | custom-call | tf_op jit(solution)/shard_map/pallas_call | solution.py:717
  81.8 0.7 copy.18
